TPU v7x, 32 devices: a whole 2x2x4 slice. The times are simulated.
32 devices in a mesh: grp: 2 (over x), sp: 4 (over z), tp: 4 (over y, core).
Axes of the slice: x: 2, y: 2, z: 4, core: 2. Of those that a mesh axis runs over, the one named last changes fastest.
Arguments:
- prompt_layer_input: bfloat16 [24, 512, 2048], P('grp', 'sp'), parts along dimension 0, may hold values from -10 to 10
- next_token_input: bfloat16 [24, 2048], P('grp'), parts along dimension 0, may hold values from -6 to 6
- value_projection: bfloat16 [2048, 2048], P(None, 'tp'), may hold values from -0.125 to 0.125
- output_gate_matrix: bfloat16 [2048, 2048], P(None, 'tp'), may hold values from -0.125 to 0.125
- key_projection: bfloat16 [2048, 256], replicated, may hold values from -0.0390625 to 0.0390625
- query_projection: bfloat16 [2048, 256], replicated, may hold values from -0.125 to 0.125
- step_projection: bfloat16 [2048, 32], replicated, may hold values from -0.125 to 0.125
- value_filter_taps: bfloat16 [4, 2048], replicated, may hold values from -3 to 3
- key_filter_taps: bfloat16 [4, 256], replicated, may hold values from -3 to 3
- query_filter_taps: bfloat16 [4, 256], replicated, may hold values from -3 to 3
- step_size_bias: float32 [32], replicated, may hold values from -4.3 to -0.7
- head_decay_logarithm: float32 [32], replicated, may hold values from -8.5 to -0.5
- direct_path_weight: float32 [32], replicated, may hold values from 0.1 to 1.9
- gated_norm_gain: float32 [32, 64], replicated, may hold values from 0.1 to 1.9
- position_decay_offset: float32 [24, 512, 32], P('grp', 'sp'), parts along dimension 0, may hold values from -2.1 to 0
Outputs:
- state_cache: bfloat16 [24, 32, 64, 128], P('grp', 'tp', 'sp'), parts along dimension 0
- first_read: bfloat16 [24, 32, 64], P('grp', 'tp', 'sp'), parts along dimension 0
There are 2 independent parts, one for each index of `grp`. A program takes and returns all parts, laid end to end along the dimension named above; an argument that names none is the same for every part. Nothing has to cross between parts.
All inputs are finite; a program needn't handle non-finite values.
Results may differ from a plain program's by a relative error of at most 0.011.
Values may be sent and summed in bfloat16 or wider, within the bound.
A program may use at most 64 MiB of HBM per device.

v0:
```python
import jax
import jax.numpy as jnp
from jax import lax
from jax.experimental import pallas as pl
from jax.experimental.pallas import tpu as pltpu
from jax.sharding import PartitionSpec as P

HEADS = 32
P_SIZE = 64
GROUPS = 2
STATE = 128
CONV = 4
SPAN = 64


epsilon = 1e-06


def shifted(block, axis, distance):
    devices = range(lax.axis_size(axis))
    route = [(i - distance, i) for i in devices if i - distance in devices]
    return lax.ppermute(block, axis, route)


def broadcast(value, axis, source):
    kept = jnp.where(lax.axis_index(axis) == source, value, 0).astype(value.dtype)
    return lax.psum(kept, axis)


def prefix(shard, axis, combine, identity):
    length, here = (lax.axis_size(axis), lax.axis_index(axis))
    everything = lax.all_gather(shard, axis)
    start = jnp.broadcast_to(jnp.asarray(identity, shard.dtype), shard.shape)

    def lap(k, before):
        at = length - 1 - k
        reached = at > here
        new = combine(before, everything[at])
        return jnp.where(reached, new, before)

    return lax.fori_loop(0, length, lap, start)


def shards(
    prompt_layer_input,
    next_token_input,
    value_projection,
    output_gate_matrix,
    key_projection,
    query_projection,
    step_projection,
    value_filter_taps,
    key_filter_taps,
    query_filter_taps,
    step_size_bias,
    head_decay_logarithm,
    direct_path_weight,
    gated_norm_gain,
    position_decay_offset,
):
    seq_count, local_len, width = prompt_layer_input.shape
    resident_heads = value_projection.shape[1] // P_SIZE
    feature_cols = resident_heads * P_SIZE
    shard_count = lax.axis_size("sp")
    rows_here = P_SIZE // shard_count
    shard_index = lax.axis_index("sp")
    leading_head = lax.axis_index("tp") * resident_heads
    group_index = leading_head // (HEADS // GROUPS)
    row_first = shard_index * rows_here
    in_cols = lax.dynamic_slice_in_dim(key_projection, group_index * STATE, STATE, 1)
    out_cols = lax.dynamic_slice_in_dim(query_projection, group_index * STATE, STATE, 1)
    weights_here = jnp.concatenate([value_projection, in_cols, out_cols], axis=1)
    step_cols = lax.dynamic_slice_in_dim(step_projection, leading_head, resident_heads, 1)
    kernel = jnp.concatenate(
        [
            lax.dynamic_slice_in_dim(value_filter_taps, leading_head * P_SIZE, feature_cols, 1),
            lax.dynamic_slice_in_dim(key_filter_taps, group_index * STATE, STATE, 1),
            lax.dynamic_slice_in_dim(query_filter_taps, group_index * STATE, STATE, 1),
        ],
        axis=1,
    ).astype(jnp.float32)
    head_decay_speed = jnp.exp(
        lax.dynamic_slice_in_dim(head_decay_logarithm, leading_head, resident_heads, 0)
    )
    bias_here = lax.dynamic_slice_in_dim(step_size_bias, leading_head, resident_heads, 0)
    skip_here = lax.dynamic_slice_in_dim(direct_path_weight, leading_head, resident_heads, 0)
    gain_here = lax.dynamic_slice(
        gated_norm_gain, (leading_head, row_first), (resident_heads, rows_here)
    )
    token_rows = prompt_layer_input.reshape(seq_count * local_len, width)
    projected = jnp.dot(token_rows, weights_here, preferred_element_type=jnp.float32).astype(
        jnp.bfloat16
    )
    projected = projected.reshape(seq_count, local_len, feature_cols + 2 * STATE)
    trailing = projected[:, local_len - (CONV - 1) :]
    before = shifted(trailing, "sp", 1)
    newest = broadcast(trailing, "sp", shard_count - 1)
    padded = jnp.concatenate([before, projected], axis=1)
    total = padded[:, 0:local_len].astype(jnp.float32) * kernel[0]
    for tap in range(1, CONV):
        total = total + padded[:, tap : tap + local_len].astype(jnp.float32) * kernel[tap]
    mixed = jax.nn.silu(total).astype(jnp.bfloat16)
    step_raw = jnp.dot(token_rows, step_cols, preferred_element_type=jnp.float32).astype(
        jnp.bfloat16
    )
    discrete_step = jax.nn.softplus(step_raw.astype(jnp.float32) + bias_here).reshape(
        seq_count, local_len, resident_heads
    )
    decay_spikes = lax.dynamic_slice_in_dim(position_decay_offset, leading_head, resident_heads, 2)
    logarithmic_decay = decay_spikes - head_decay_speed * discrete_step
    block_count = local_len // SPAN
    cumulative = jnp.cumsum(
        logarithmic_decay.reshape(seq_count, block_count, SPAN, resident_heads), axis=2
    )
    decay_weight = jnp.exp(cumulative[:, :, -1:] - cumulative) * discrete_step.reshape(
        seq_count, block_count, SPAN, resident_heads
    )
    head_input = mixed[:, :, :feature_cols].reshape(
        seq_count, block_count, SPAN, resident_heads, P_SIZE
    )
    weighted = (head_input.astype(jnp.float32) * decay_weight[..., None]).astype(jnp.bfloat16)
    in_map = mixed[:, :, feature_cols : feature_cols + STATE].reshape(
        seq_count, block_count, SPAN, STATE
    )
    block_state = jnp.einsum(
        "bcshp,bcsn->bchpn", weighted, in_map, preferred_element_type=jnp.float32
    )
    block_log = cumulative[:, :, -1]
    own_log = jnp.sum(block_log, axis=1)
    after_block = jnp.exp(own_log[:, None] - jnp.cumsum(block_log, axis=1))
    local_state = jnp.sum(after_block[..., None, None] * block_state, axis=1)
    later_log = prefix(own_log, "sp", jnp.add, jnp.zeros_like(own_log))
    scaled = jnp.exp(later_log)[:, :, None, None] * local_state
    own_rows = lax.psum_scatter(scaled, "sp", scatter_dimension=2, tiled=True)
    state_cache = own_rows.astype(jnp.bfloat16)
    new_raw = jnp.dot(next_token_input, weights_here, preferred_element_type=jnp.float32).astype(
        jnp.bfloat16
    )
    new_step = jnp.dot(next_token_input, step_cols, preferred_element_type=jnp.float32).astype(
        jnp.bfloat16
    )
    new_gate = jnp.dot(
        next_token_input, output_gate_matrix, preferred_element_type=jnp.float32
    ).astype(jnp.bfloat16)
    window = jnp.concatenate([newest, new_raw[:, None]], axis=1)
    new_mixed = jax.nn.silu(jnp.sum(window.astype(jnp.float32) * kernel[None], axis=1)).astype(
        jnp.bfloat16
    )
    new_input = lax.dynamic_slice_in_dim(
        new_mixed[:, :feature_cols].reshape(seq_count, resident_heads, P_SIZE),
        row_first,
        rows_here,
        2,
    ).astype(jnp.float32)
    new_in = new_mixed[:, feature_cols : feature_cols + STATE].astype(jnp.float32)
    new_out = new_mixed[:, feature_cols + STATE :].astype(jnp.float32)
    new_step_size = jax.nn.softplus(new_step.astype(jnp.float32) + bias_here)
    cache_values = lax.optimization_barrier(state_cache).astype(jnp.float32)
    new_state = (
        jnp.exp(-head_decay_speed * new_step_size)[:, :, None, None] * cache_values
        + (new_step_size[:, :, None] * new_input)[..., None] * new_in[:, None, None, :]
    )
    readout = (
        jnp.sum(new_state * new_out[:, None, None, :], axis=-1)
        + skip_here[None, :, None] * new_input
    )
    gate_rows = lax.dynamic_slice_in_dim(
        new_gate.reshape(seq_count, resident_heads, P_SIZE), row_first, rows_here, 2
    )
    gated = readout * jax.nn.silu(gate_rows.astype(jnp.float32))
    squares = lax.psum(jnp.sum(gated * gated, axis=(1, 2)), ("sp", "tp"))
    scale = lax.rsqrt(squares / (HEADS * P_SIZE) + epsilon)
    first_read = (gated * scale[:, None, None] * gain_here[None]).astype(jnp.bfloat16)
    return (state_cache, first_read)


F32, BF16 = jnp.float32, jnp.bfloat16
MESH = pl.DeviceIdType.MESH
EXACT = lax.Precision.HIGHEST


def exact_dot(a, b, dims=((1,), (0,))):
    return lax.dot_general(a, b, (dims, ((), ())), precision=EXACT, preferred_element_type=F32)


def softplus(v):
    return jnp.maximum(v, 0.0) + jnp.log1p(jnp.exp(-jnp.abs(v)))


def silu(v):
    return v / (1.0 + jnp.exp(-v))


def ones_where(shape, test, dtype=F32):
    rows = lax.broadcasted_iota(jnp.int32, shape, 0)
    cols = lax.broadcasted_iota(jnp.int32, shape, 1)
    return jnp.where(test(rows, cols), 1.0, 0.0).astype(dtype)


def mixer_kernel(
    dims,
    x_hbm,
    next_ref,
    wv_hbm,
    wg_hbm,
    wk_hbm,
    wq_hbm,
    ws_hbm,
    tv_ref,
    tk_ref,
    tq_ref,
    bias_ref,
    speed_ref,
    skip_ref,
    gain_ref,
    off_hbm,
    cache_ref,
    read_ref,
    xbuf,
    edge,
    wall,
    wq,
    ws,
    wg,
    off,
    taps,
    pad,
    halo_out,
    halo_in,
    halo,
    newest,
    logs_out,
    logs,
    sendbuf,
    recv,
    sq_out,
    sq_in,
    expand,
    load_sem,
    x_sem,
    halo_sem,
    new_send,
    new_recv,
    st_send,
    st_recv,
    log_send,
    log_recv,
    sq_send,
    sq_recv,
):
    n, m, S, L, heads, R, G = dims
    F = heads * P_SIZE
    C = F + STATE
    SP = sq_out.shape[0]
    steps = S // G
    me, tp = lax.axis_index("sp"), lax.axis_index("tp")
    lead = tp * heads
    group = lax.div(lead, HEADS // GROUPS)
    fcol = pl.multiple_of(tp * F, 128)
    gcol = pl.multiple_of(group * STATE, 128)

    def load(src, dst, k):
        c = pltpu.make_async_copy(src, dst, load_sem.at[k])
        c.start()
        return c

    def load_x(g):
        return pltpu.make_async_copy(
            x_hbm.at[pl.ds(g * G, G)], xbuf.at[pl.ds(g * G, G)], x_sem.at[g]
        )

    first = [
        load(x_hbm.at[:, pl.ds(L - 16, 16)], edge.at[pl.ds(0, S)], 0),
        load(wk_hbm.at[:, pl.ds(gcol, STATE)], wall.at[:, pl.ds(F, STATE)], 1),
        load(ws_hbm, ws, 2),
        load(wq_hbm.at[:, pl.ds(gcol, STATE)], wq, 3),
        load(wv_hbm, wall.at[:, pl.ds(0, F)], 4),
    ]
    for g in range(steps):
        load_x(g).start()
    off_load = load(off_hbm, off, 5)
    gate_load = load(wg_hbm, wg, 6)

    peers = [(a, b) for a in range(n) for b in range(m) if (a, b) != (0, 0)]

    def at(a, b=0):
        return {"sp": lax.rem(me + a, n), "tp": lax.rem(tp + b, m)}

    barrier = pltpu.get_barrier_semaphore()
    for a, b in peers:
        pl.semaphore_signal(barrier, inc=1, device_id=at(a, b), device_id_type=MESH)

    taps[:, 0:F] = tv_ref[:, pl.ds(fcol, F)].astype(F32)
    taps[:, F:C] = tk_ref[:, pl.ds(gcol, STATE)].astype(F32)
    taps[:, C : C + STATE] = tq_ref[:, pl.ds(gcol, STATE)].astype(F32)
    edge[S] = jnp.zeros(edge.shape[1:], BF16)
    edge[S, 0:S, :] = next_ref[...]
    halo_out[...] = jnp.zeros_like(halo_out)
    newest_zero = jnp.zeros(newest.shape[1:], F32)
    head_of = ones_where((HEADS, F), lambda i, c: i == lead + lax.div(c, P_SIZE), BF16)
    expand[0:HEADS, :] = head_of
    expand[HEADS : 2 * HEADS, :] = head_of
    bias = bias_ref[...]
    speed = jnp.exp(speed_ref[...])
    square = jnp.zeros((128, 128 - HEADS), F32)

    def columns(row):
        full = jnp.concatenate([jnp.broadcast_to(row, (128, HEADS)), square], axis=1)
        return full.T[0:HEADS]

    bias_t, speed_t = columns(bias), columns(speed)

    for c in first:
        c.wait()
    wall[:, C : C + STATE] = jnp.concatenate(
        [ws[...], jnp.zeros((STATE - HEADS, ws.shape[1]), BF16)], axis=0
    ).T
    rows = edge[...].reshape((S + 1) * 16, edge.shape[2])
    eproj = jnp.dot(rows, wall[...], preferred_element_type=F32).astype(BF16).astype(F32)
    eq = jnp.dot(rows, wq[...], preferred_element_type=F32).astype(BF16).astype(F32)
    e3 = eproj.reshape(S + 1, 16, C + STATE)
    q3 = eq.reshape(S + 1, 16, STATE)
    total = jnp.zeros((S, C + STATE), F32)
    for j in range(CONV - 1):
        row = 16 - (CONV - 1) + j
        tail = e3[0:S, row, 0:C]
        halo_out[j, 0:S, :] = tail.astype(BF16)
        total = total + jnp.concatenate([tail, q3[0:S, row, :]], axis=1) * taps[j : j + 1, :]
    new_raw = jnp.concatenate([e3[S, :, 0:C], q3[S]], axis=1)
    new_step = e3[S, :, C : C + HEADS]

    pl.semaphore_wait(barrier, len(peers))

    def halo_copy():
        return pltpu.make_async_remote_copy(
            halo_out, halo_in, halo_sem.at[0], halo_sem.at[1], device_id=at(1), device_id_type=MESH
        )

    @pl.when(me < n - 1)
    def _():
        halo_copy().start()

    def newest_copy(k):
        return pltpu.make_async_remote_copy(
            newest, newest, new_send.at[k], new_recv, device_id=at(k), device_id_type=MESH
        )

    @pl.when(me == n - 1)
    def _():
        newest[0] = newest_zero
        newest[0, 0:S, :] = total
        for k in range(1, n):
            newest_copy(k).start()

    def state_copy(g, k):
        to = lax.rem(me + k, n)
        return pltpu.make_async_remote_copy(
            sendbuf.at[to, pl.ds(g * G, G)],
            recv.at[me, pl.ds(g * G, G)],
            st_send.at[g, k],
            st_recv.at[g, k],
            device_id=at(k),
            device_id_type=MESH,
        )

    def log_copy(g, k):
        return pltpu.make_async_remote_copy(
            logs_out.at[pl.ds(g * G, G)],
            logs.at[me, pl.ds(g * G, G)],
            log_send.at[g, k],
            log_recv.at[g, k],
            device_id=at(k),
            device_id_type=MESH,
        )

    off_load.wait()
    later_ones = ones_where((L, L), lambda u, t: u > t)

    def step(g, carry):
        load_x(g).wait()
        xg = xbuf[pl.ds(g * G, G)].reshape(G * L, xbuf.shape[2])
        acc = jnp.dot(xg, wall[...], preferred_element_type=F32).astype(BF16).astype(F32)

        @pl.when(g == 0)
        def _():
            @pl.when(me == 0)
            def _():
                halo[...] = jnp.zeros_like(halo)

            @pl.when(me > 0)
            def _():
                halo_copy().wait_recv()
                halo[...] = halo_in[...].astype(F32)

        for q in range(G):
            p = g * G + q
            raw = acc[q * L : (q + 1) * L]
            pad[q, 8 : 8 + L, :] = raw[:, 0:C]
            for j in range(CONV - 1):
                r = 8 - (CONV - 1) + j
                pad[q, r : r + 1, :] = halo[j, pl.ds(p, 1), :]
            dt = softplus(raw[:, C : C + STATE].T[0:HEADS] + bias_t)
            ld = off[p] - speed_t * dt
            suffix = exact_dot(ld, later_ones)
            own = jnp.broadcast_to(suffix[:, 0:1] + ld[:, 0:1], (HEADS, 128))
            logs_out[p] = jnp.concatenate([own] * (128 // HEADS), axis=0).T[0:8]
            w = dt * jnp.exp(suffix)
            hi = w.astype(BF16)
            lo = (w - hi.astype(F32)).astype(BF16)
            wide = lax.dot_general(
                jnp.concatenate([hi, lo], axis=0),
                expand[...],
                (((0,), (0,)), ((), ())),
                preferred_element_type=F32,
            )

            def mixed(c):
                s = slice(c, c + 128)
                t = pad[q, 8 - (CONV - 1) : 8 - (CONV - 1) + L, s] * taps[0:1, s]
                for j in range(1, CONV):
                    r = 8 - (CONV - 1) + j
                    t = t + pad[q, r : r + L, s] * taps[j : j + 1, s]
                return silu(t).astype(BF16)

            in_map = mixed(F)
            for c in range(0, F, 128):
                weighted = (mixed(c).astype(F32) * wide[:, c : c + 128]).astype(BF16)
                share = lax.dot_general(
                    weighted, in_map, (((0,), (0,)), ((), ())), preferred_element_type=F32
                ).astype(BF16)
                for hh in range(128 // P_SIZE):
                    h = c // P_SIZE + hh
                    for d in range(n):
                        b = hh * P_SIZE + d * R
                        sendbuf[d, p, h * R : (h + 1) * R, :] = share[b : b + R]
        for k in range(1, n):
            log_copy(g, k).start()
        for k in range(1, n):
            state_copy(g, k).start()
        return carry

    lax.fori_loop(0, steps, step, 0)

    logs[me] = logs_out[...]
    recv[me] = sendbuf[me]

    RH = heads * R
    head_rows = ones_where((RH, HEADS), lambda l, i: i == lead + lax.div(l, R))
    head_cols = ones_where((HEADS, RH), lambda i, l: i == lead + lax.div(l, R))
    pick = ones_where(
        (F, RH), lambda c, l: c == lax.div(l, R) * P_SIZE + me * R + lax.rem(l, R), BF16
    )
    row_pick = ones_where((P_SIZE, RH), lambda c, l: c == me * R + lax.rem(l, R))
    gate_load.wait()
    gate = jnp.dot(edge[S], wg[...], preferred_element_type=F32).astype(BF16)
    gate_here = silu(jnp.dot(gate, pick, preferred_element_type=F32))
    gain_here = jnp.sum(exact_dot(gain_ref[...], row_pick) * head_cols, axis=0, keepdims=True)
    skip_here = exact_dot(skip_ref[...], head_cols)
    new_dt = softplus(new_step + bias)
    dt_here = exact_dot(new_dt, head_cols)
    keep_here = jnp.exp(-exact_dot(speed * new_dt, head_cols))

    @pl.when(me < n - 1)
    def _():
        pltpu.make_async_remote_copy(
            newest, newest, new_send.at[0], new_recv, device_id=at(1), device_id_type=MESH
        ).wait_recv()

    new_mixed = silu(newest[0] + new_raw * taps[CONV - 1 : CONV, :]).astype(BF16)
    new_input = jnp.dot(new_mixed[:, 0:F], pick, preferred_element_type=F32)
    new_in = new_mixed[:, F:C].astype(F32)
    new_out = new_mixed[:, C : C + STATE]
    both = jnp.sum(new_in * new_out.astype(F32), axis=1, keepdims=True)

    where_row = lax.broadcasted_iota(jnp.int32, (SP, RH), 0)
    y = jnp.zeros((SP, RH), F32)
    for g in range(steps):
        for k in range(1, n):
            log_copy(g, k).wait_recv()
            state_copy(g, k).wait_recv()
        for p in range(g * G, (g + 1) * G):
            later = jnp.zeros((1, HEADS), F32)
            tot = jnp.zeros((RH, STATE), F32)
            for s in reversed(range(n)):
                factor = jnp.sum(head_rows * jnp.exp(later), axis=1, keepdims=True)
                tot = tot + factor * recv[s, p].astype(F32)
                later = later + logs[s, p, 0:1, 0:HEADS]
            kept = tot.astype(BF16)
            cache_ref[p] = kept
            part = lax.dot_general(
                new_out, kept, (((1,), (1,)), ((), ())), preferred_element_type=F32
            )
            y = jnp.where(where_row == p, part, y)
    readout = keep_here * y + dt_here * new_input * both + skip_here * new_input
    gated = readout * gate_here
    sq = jnp.broadcast_to(jnp.sum(gated * gated, axis=1, keepdims=True), sq_out.shape)
    sq_out[...] = sq

    def sq_copy(i):
        a, b = peers[i]
        return pltpu.make_async_remote_copy(
            sq_out, sq_in.at[i], sq_send.at[i], sq_recv.at[i], device_id=at(a, b), device_id_type=MESH
        )

    for i in range(len(peers)):
        sq_copy(i).start()
    for i in range(len(peers)):
        sq_copy(i).wait_recv()
        sq = sq + sq_in[i]
    scale = lax.rsqrt(sq[:, 0:1] / (HEADS * P_SIZE) + epsilon)
    read_ref[...] = (gated * scale * gain_here).astype(BF16)[0:S]

    for i in range(len(peers)):
        sq_copy(i).wait_send()
    for k in range(1, n):
        for g in range(steps):
            log_copy(g, k).wait_send()
            state_copy(g, k).wait_send()

    @pl.when(me < n - 1)
    def _():
        halo_copy().wait_send()

    @pl.when(me == n - 1)
    def _():
        for k in range(1, n):
            newest_copy(k).wait_send()


def fused(*args):
    x, wv, wk = args[0], args[2], args[4]
    S, L, D = x.shape
    n, m = lax.axis_size("sp"), lax.axis_size("tp")
    F = wv.shape[1]
    heads = F // P_SIZE
    R = P_SIZE // n
    G = next(g for g in (2, 3, 1) if S % g == 0)
    steps = S // G
    C, RH, SP = F + STATE, heads * R, 16
    dims = (n, m, S, L, heads, R, G)
    flat = list(args)
    for i in (10, 11, 12):
        flat[i] = args[i].reshape(1, HEADS)
    flat[6] = args[6].T
    flat[14] = jnp.swapaxes(args[14], 1, 2)
    hbm, vmem = pl.BlockSpec(memory_space=pl.ANY), pl.BlockSpec(memory_space=pltpu.VMEM)
    specs = [hbm, vmem, hbm, hbm, hbm, hbm, hbm] + [vmem] * 7 + [hbm]
    dma = pltpu.SemaphoreType.DMA
    cache, read = pl.pallas_call(
        lambda *refs: mixer_kernel(dims, *refs),
        out_shape=(
            jax.ShapeDtypeStruct((S, RH, STATE), BF16),
            jax.ShapeDtypeStruct((S, RH), BF16),
        ),
        in_specs=specs,
        out_specs=(vmem, vmem),
        scratch_shapes=[
            pltpu.VMEM((S, L, D), BF16),
            pltpu.VMEM((S + 1, 16, D), BF16),
            pltpu.VMEM((D, C + STATE), BF16),
            pltpu.VMEM((D, STATE), BF16),
            pltpu.VMEM((HEADS, D), BF16),
            pltpu.VMEM((D, F), BF16),
            pltpu.VMEM((S, HEADS, L), F32),
            pltpu.VMEM((CONV, C + STATE), F32),
            pltpu.VMEM((G, 8 + L, C), F32),
            pltpu.VMEM((CONV - 1, SP, C), BF16),
            pltpu.VMEM((CONV - 1, SP, C), BF16),
            pltpu.VMEM((CONV - 1, SP, C), F32),
            pltpu.VMEM((1, SP, C + STATE), F32),
            pltpu.VMEM((S, 8, 128), F32),
            pltpu.VMEM((n, S, 8, 128), F32),
            pltpu.VMEM((n, S, RH, STATE), BF16),
            pltpu.VMEM((n, S, RH, STATE), BF16),
            pltpu.VMEM((SP, 128), F32),
            pltpu.VMEM((n * m - 1, SP, 128), F32),
            pltpu.VMEM((2 * HEADS, F), BF16),
            dma((7,)),
            dma((steps,)),
            dma((2,)),
            dma((n,)),
            dma,
            dma((steps, n)),
            dma((steps, n)),
            dma((steps, n)),
            dma((steps, n)),
            dma((n * m,)),
            dma((n * m,)),
        ],
        compiler_params=pltpu.CompilerParams(
            collective_id=0, has_side_effects=True, vmem_limit_bytes=56 * 1024 * 1024
        ),
    )(*flat)
    return cache.reshape(S, heads, R, STATE), read.reshape(S, heads, R)


def fits(n, m, shapes):
    (S, L), F = shapes
    heads, R = F // P_SIZE, P_SIZE // n
    return (
        n > 1
        and F % 128 == 0
        and R % 16 == 0
        and (heads * R) % 128 == 0
        and S <= 16
        and L % 16 == 0
        and L == 128
        and (HEADS // GROUPS) % heads == 0
    )


def part(*args):
    shapes = (args[0].shape[:2], args[2].shape[1])
    if fits(lax.axis_size("sp"), lax.axis_size("tp"), shapes):
        return fused(*args)
    return shards(*args)


def solution(mesh):
    in_specs = (
        P("grp", "sp", None),
        P("grp", None),
        P(None, "tp"),
        P(None, "tp"),
        P(),
        P(),
        P(),
        P(),
        P(),
        P(),
        P(),
        P(),
        P(),
        P(),
        P("grp", "sp", None),
    )
    out_specs = (P("grp", "tp", "sp", None), P("grp", "tp", "sp"))
    return jax.shard_map(part, mesh=mesh, in_specs=in_specs, out_specs=out_specs, check_vma=False)
```

profile of v0, /device:TPU:0, one launch (start us, length us, event | category | flops | bytes accessed | tf_op | source)
XLA Modules:
  0.0 61.9 jit_solution(5423331118877304753)
XLA Ops:
  0.6 58.1 %shard_map.158 = (bf16[12,128,128]{2,1,0:T(8,128)(2,1)}, bf16[12,128]{1,0:T(8,128)(2,1)}) custom-call(bf16[12,128,2048]{2,1,0:T(8,128)(2,1)} %refs_0_.1, bf16[12,2048]{1,0:T(8,128)(2,1)} %refs_1_.1, bf16[2048,512]{1,0:T(8,128)(2,1)} %refs_2_.1, bf16[2048,512]{1,0:T(8,128)(2,1)} %refs_3_.1, bf16[2048,256]{1,0:T(8,128)(2,1)} %refs_4_.1, ...), custom_call_target="tpu_custom_call" | custom-call | tf_op jit(solution)/shard_map/pallas_call | solution.py:549
  58.8 1.4 %reshape.23 = bf16[12,8,16]{2,1,0:T(8,128)(2,1)} reshape(bf16[12,128]{1,0:T(8,128)(2,1)} %get-tuple-element.5) | data formatting | bytes 6144 | tf_op jit(solution)/shard_map/reshape | solution.py:594
  60.2 1.8 %copy.18 = bf16[12,8,16,128]{3,2,1,0:T(8,128)(2,1)} copy(bf16[12,8,16,128]{3,2,1,0:T(8,128)(2,1)} %bitcast.6) | data formatting | bytes 786432
where the time goes:
time: 62.2 us; the launch traced here: 61.9 us
  Pallas kernels  58.1 us (93%)
  local copies, waits for them, and re-layouts  3.14 us (5%)
  between operations  0.64 us (1%)
    pallas_call x1, Pallas kernels, fused(): pl.pallas_call(lambda *refs: mixer_kernel(dims, *refs), out_shape=(jax.Sh...  58.1 us
    unnamed x1, local copies, waits for them, and re-layouts  1.77 us
    reshape x1, local copies, waits for them, and re-layouts, fused(): return (cache.reshape(S, heads, R, STATE), read.reshape(S, heads, R))  1.37 us

commit v1 on v0

--- a/solution.py
+++ b/solution.py
@@ -214,7 +214,7 @@
     skip_ref,
     gain_ref,
     off_hbm,
-    cache_ref,
+    cache_hbm,
     read_ref,
     xbuf,
     edge,
@@ -225,36 +225,44 @@
     off,
     taps,
     pad,
+    wsplit,
     halo_out,
     halo_in,
     halo,
     newest,
-    logs_out,
-    logs,
-    sendbuf,
-    recv,
+    heads_t,
+    decay,
+    log_own,
+    log_out,
+    log_in,
+    own,
+    from_left,
+    from_right,
+    kept_buf,
     sq_out,
     sq_in,
     expand,
     load_sem,
     x_sem,
     halo_sem,
-    new_send,
-    new_recv,
+    new_sem,
     st_send,
     st_recv,
     log_send,
     log_recv,
+    out_sem,
     sq_send,
     sq_recv,
 ):
     n, m, S, L, heads, R, G = dims
     F = heads * P_SIZE
     C = F + STATE
-    SP = sq_out.shape[0]
+    RH = heads * R
+    SP = 16
     steps = S // G
+    lead_steps = min(LEAD, steps)
     me, tp = lax.axis_index("sp"), lax.axis_index("tp")
-    lead = tp * heads
+    lead = pl.multiple_of(tp * heads, 8)
     group = lax.div(lead, HEADS // GROUPS)
     fcol = pl.multiple_of(tp * F, 128)
     gcol = pl.multiple_of(group * STATE, 128)
@@ -270,15 +278,15 @@
         )
 
     first = [
-        load(x_hbm.at[:, pl.ds(L - 16, 16)], edge.at[pl.ds(0, S)], 0),
-        load(wk_hbm.at[:, pl.ds(gcol, STATE)], wall.at[:, pl.ds(F, STATE)], 1),
-        load(ws_hbm, ws, 2),
-        load(wq_hbm.at[:, pl.ds(gcol, STATE)], wq, 3),
-        load(wv_hbm, wall.at[:, pl.ds(0, F)], 4),
+        load(ws_hbm.at[pl.ds(lead, heads), :], ws, 0),
+        load(x_hbm.at[:, pl.ds(L - 16, 16)], edge.at[pl.ds(0, S)], 1),
+        load(wk_hbm.at[:, pl.ds(gcol, STATE)], wall.at[:, pl.ds(F, STATE)], 2),
+        load(wv_hbm, wall.at[:, pl.ds(0, F)], 3),
+        load(wq_hbm.at[:, pl.ds(gcol, STATE)], wq, 4),
     ]
+    off_load = load(off_hbm.at[:, pl.ds(lead, heads), :], off, 5)
     for g in range(steps):
         load_x(g).start()
-    off_load = load(off_hbm, off, 5)
     gate_load = load(wg_hbm, wg, 6)
 
     peers = [(a, b) for a in range(n) for b in range(m) if (a, b) != (0, 0)]
@@ -296,38 +304,42 @@
     edge[S] = jnp.zeros(edge.shape[1:], BF16)
     edge[S, 0:S, :] = next_ref[...]
     halo_out[...] = jnp.zeros_like(halo_out)
-    newest_zero = jnp.zeros(newest.shape[1:], F32)
-    head_of = ones_where((HEADS, F), lambda i, c: i == lead + lax.div(c, P_SIZE), BF16)
-    expand[0:HEADS, :] = head_of
-    expand[HEADS : 2 * HEADS, :] = head_of
+    head_of = ones_where((heads, F), lambda i, c: i == lax.div(c, P_SIZE))
+    expand[...] = jnp.concatenate([head_of, head_of], axis=0).astype(BF16)
     bias = bias_ref[...]
     speed = jnp.exp(speed_ref[...])
     square = jnp.zeros((128, 128 - HEADS), F32)
 
-    def columns(row):
+    def columns(row, k):
         full = jnp.concatenate([jnp.broadcast_to(row, (128, HEADS)), square], axis=1)
-        return full.T[0:HEADS]
-
-    bias_t, speed_t = columns(bias), columns(speed)
-
-    for c in first:
+        heads_t[k] = full.T[0:HEADS]
+        return heads_t[k, pl.ds(lead, heads), :]
+
+    bias_t, speed_t = columns(bias, 0), columns(speed, 1)
+
+    @pl.when(me == 0)
+    def _():
+        from_left[:, 0] = jnp.zeros((S, RH, STATE), BF16)
+
+    @pl.when(me == n - 1)
+    def _():
+        from_right[:, n - 1] = jnp.zeros((S, RH, STATE), BF16)
+        log_in[...] = jnp.zeros_like(log_in)
+
+    eye = ones_where((heads, 128), lambda i, c: i == c)
+    later_ones = ones_where((L, L), lambda u, t: u > t, BF16)
+
+    first[0].wait()
+    wall[:, C : C + STATE] = jnp.concatenate(
+        [ws[...], jnp.zeros((STATE - heads, ws.shape[1]), BF16)], axis=0
+    ).T
+    for c in first[1:4]:
         c.wait()
-    wall[:, C : C + STATE] = jnp.concatenate(
-        [ws[...], jnp.zeros((STATE - HEADS, ws.shape[1]), BF16)], axis=0
-    ).T
     rows = edge[...].reshape((S + 1) * 16, edge.shape[2])
     eproj = jnp.dot(rows, wall[...], preferred_element_type=F32).astype(BF16).astype(F32)
-    eq = jnp.dot(rows, wq[...], preferred_element_type=F32).astype(BF16).astype(F32)
     e3 = eproj.reshape(S + 1, 16, C + STATE)
-    q3 = eq.reshape(S + 1, 16, STATE)
-    total = jnp.zeros((S, C + STATE), F32)
     for j in range(CONV - 1):
-        row = 16 - (CONV - 1) + j
-        tail = e3[0:S, row, 0:C]
-        halo_out[j, 0:S, :] = tail.astype(BF16)
-        total = total + jnp.concatenate([tail, q3[0:S, row, :]], axis=1) * taps[j : j + 1, :]
-    new_raw = jnp.concatenate([e3[S, :, 0:C], q3[S]], axis=1)
-    new_step = e3[S, :, C : C + HEADS]
+        halo_out[j, 0:S, :] = e3[0:S, 16 - (CONV - 1) + j, 0:C].astype(BF16)
 
     pl.semaphore_wait(barrier, len(peers))
 
@@ -340,75 +352,101 @@
     def _():
         halo_copy().start()
 
-    def newest_copy(k):
+    first[4].wait()
+    eq = jnp.dot(rows, wq[...], preferred_element_type=F32).astype(BF16).astype(F32)
+    q3 = eq.reshape(S + 1, 16, STATE)
+    new_raw = jnp.concatenate([e3[S, :, 0:C], q3[S]], axis=1)
+    new_step = e3[S, :, C : C + STATE]
+
+    def newest_copy():
         return pltpu.make_async_remote_copy(
-            newest, newest, new_send.at[k], new_recv, device_id=at(k), device_id_type=MESH
+            newest,
+            newest,
+            new_sem.at[0],
+            new_sem.at[1],
+            device_id=at(n - 1),
+            device_id_type=MESH,
         )
 
     @pl.when(me == n - 1)
     def _():
-        newest[0] = newest_zero
-        newest[0, 0:S, :] = total
-        for k in range(1, n):
-            newest_copy(k).start()
-
-    def state_copy(g, k):
-        to = lax.rem(me + k, n)
+        total = jnp.zeros((S, C + STATE), F32)
+        for j in range(CONV - 1):
+            row = 16 - (CONV - 1) + j
+            tail = jnp.concatenate([e3[0:S, row, 0:C], q3[0:S, row, :]], axis=1)
+            total = total + tail * taps[j : j + 1, :]
+        newest[...] = jnp.zeros_like(newest)
+        newest[0:S, :] = total
+        newest_copy().start()
+
+    def span(s, right, far):
+        if right:
+            return (s + 2, n) if far else (s + 1, s + 2)
+        return (0, s - 1) if far else (s - 1, s)
+
+    def flow(g, s, right, far):
+        lo, hi = span(s, right, far)
+        if not (0 <= lo < hi <= n):
+            return None
+        k = 2 * int(right) + int(far)
+        here = (pl.ds(g * G, G), pl.ds(lo, hi - lo))
         return pltpu.make_async_remote_copy(
-            sendbuf.at[to, pl.ds(g * G, G)],
-            recv.at[me, pl.ds(g * G, G)],
-            st_send.at[g, k],
-            st_recv.at[g, k],
-            device_id=at(k),
+            own.at[here],
+            (from_left if right else from_right).at[here],
+            st_send.at[k, g],
+            st_recv.at[k, g],
+            device_id=at(1 if right else n - 1),
             device_id_type=MESH,
         )
 
-    def log_copy(g, k):
+    def begin(g, s, right, far):
+        c = flow(g, s, right, far)
+        if c is not None:
+            c.start()
+
+    def log_copy(g):
+        here = pl.ds(g * G, G)
         return pltpu.make_async_remote_copy(
-            logs_out.at[pl.ds(g * G, G)],
-            logs.at[me, pl.ds(g * G, G)],
-            log_send.at[g, k],
-            log_recv.at[g, k],
-            device_id=at(k),
+            log_out.at[here],
+            log_in.at[here],
+            log_send.at[g],
+            log_recv.at[g],
+            device_id=at(n - 1),
             device_id_type=MESH,
         )
 
-    off_load.wait()
-    later_ones = ones_where((L, L), lambda u, t: u > t)
-
-    def step(g, carry):
+    def project(g):
         load_x(g).wait()
+        slot = lax.rem(g, lead_steps)
         xg = xbuf[pl.ds(g * G, G)].reshape(G * L, xbuf.shape[2])
         acc = jnp.dot(xg, wall[...], preferred_element_type=F32).astype(BF16).astype(F32)
-
-        @pl.when(g == 0)
-        def _():
-            @pl.when(me == 0)
-            def _():
-                halo[...] = jnp.zeros_like(halo)
-
-            @pl.when(me > 0)
-            def _():
-                halo_copy().wait_recv()
-                halo[...] = halo_in[...].astype(F32)
-
         for q in range(G):
             p = g * G + q
             raw = acc[q * L : (q + 1) * L]
-            pad[q, 8 : 8 + L, :] = raw[:, 0:C]
+            pad[slot, q, 8 : 8 + L, :] = raw[:, 0:C]
+            dt = softplus(raw[:, C : C + STATE].T[0:heads] + bias_t)
+            ld = off[p] - speed_t * dt
+            a = ld.astype(BF16).astype(F32)
+            b = (ld - a).astype(BF16).astype(F32)
+            parts = jnp.concatenate([a, b, ld - a - b, jnp.zeros_like(a)], axis=0).astype(BF16)
+            sums = jnp.dot(parts, later_ones, preferred_element_type=F32)
+            suffix = sums[0:heads] + sums[heads : 2 * heads] + sums[2 * heads : 3 * heads]
+            whole = jnp.broadcast_to(suffix[:, 0:1] + ld[:, 0:1], (heads, 128))
+            decay[p] = jnp.exp(whole)
+            log_own[p] = jnp.sum(whole * eye, axis=0, keepdims=True)
+            w = dt * jnp.exp(suffix)
+            hi = w.astype(BF16).astype(F32)
+            wsplit[slot, q] = jnp.concatenate([hi, w - hi], axis=0).astype(BF16)
+
+    def states(g):
+        slot = lax.rem(g, lead_steps)
+        for q in range(G):
+            p = g * G + q
             for j in range(CONV - 1):
                 r = 8 - (CONV - 1) + j
-                pad[q, r : r + 1, :] = halo[j, pl.ds(p, 1), :]
-            dt = softplus(raw[:, C : C + STATE].T[0:HEADS] + bias_t)
-            ld = off[p] - speed_t * dt
-            suffix = exact_dot(ld, later_ones)
-            own = jnp.broadcast_to(suffix[:, 0:1] + ld[:, 0:1], (HEADS, 128))
-            logs_out[p] = jnp.concatenate([own] * (128 // HEADS), axis=0).T[0:8]
-            w = dt * jnp.exp(suffix)
-            hi = w.astype(BF16)
-            lo = (w - hi.astype(F32)).astype(BF16)
+                pad[slot, q, r : r + 1, :] = halo[j, pl.ds(p, 1), :]
             wide = lax.dot_general(
-                jnp.concatenate([hi, lo], axis=0),
+                wsplit[slot, q],
                 expand[...],
                 (((0,), (0,)), ((), ())),
                 preferred_element_type=F32,
@@ -416,10 +454,10 @@
 
             def mixed(c):
                 s = slice(c, c + 128)
-                t = pad[q, 8 - (CONV - 1) : 8 - (CONV - 1) + L, s] * taps[0:1, s]
+                t = pad[slot, q, 8 - (CONV - 1) : 8 - (CONV - 1) + L, s] * taps[0:1, s]
                 for j in range(1, CONV):
                     r = 8 - (CONV - 1) + j
-                    t = t + pad[q, r : r + L, s] * taps[j : j + 1, s]
+                    t = t + pad[slot, q, r : r + L, s] * taps[j : j + 1, s]
                 return silu(t).astype(BF16)
 
             in_map = mixed(F)
@@ -432,21 +470,115 @@
                     h = c // P_SIZE + hh
                     for d in range(n):
                         b = hh * P_SIZE + d * R
-                        sendbuf[d, p, h * R : (h + 1) * R, :] = share[b : b + R]
-        for k in range(1, n):
-            log_copy(g, k).start()
-        for k in range(1, n):
-            state_copy(g, k).start()
+                        own[p, d, h * R : (h + 1) * R, :] = share[b : b + R]
+
+    def later_factor(p):
+        row = jnp.sum(eye * log_in[p], axis=1, keepdims=True)
+        return jnp.exp(jnp.broadcast_to(row, (heads, 128)))
+
+    def relay(g):
+        for s in range(1, n - 1):
+
+            @pl.when(me == s)
+            def _(s=s):
+                if s + 1 < n:
+                    flow(g, s - 1, True, True).wait_recv()
+                for q in range(G):
+                    p = g * G + q
+                    factor = decay[p]
+                    for d in range(s + 1, n):
+                        for h in range(heads):
+                            z = (p, d, slice(h * R, (h + 1) * R))
+                            got = from_left[z].astype(F32) * factor[h : h + 1, :]
+                            own[z] = (own[z].astype(F32) + got).astype(BF16)
+                begin(g, s, True, True)
+                begin(g, s, True, False)
+                log_copy(g).wait_recv()
+                for q in range(G):
+                    p = g * G + q
+                    log_out[p] = log_in[p] + log_own[p]
+                log_copy(g).start()
+                flow(g, s + 1, False, True).wait_recv()
+                for q in range(G):
+                    p = g * G + q
+                    factor = later_factor(p)
+                    for d in range(s):
+                        for h in range(heads):
+                            z = (p, d, slice(h * R, (h + 1) * R))
+                            mine = own[z].astype(F32) * factor[h : h + 1, :]
+                            own[z] = (from_right[z].astype(F32) + mine).astype(BF16)
+                begin(g, s, False, True)
+                begin(g, s, False, False)
+
+    off_load.wait()
+    lax.fori_loop(0, lead_steps, lambda g, carry: (project(g), carry)[1], 0)
+
+    @pl.when(me == 0)
+    def _():
+        halo[...] = jnp.zeros_like(halo)
+
+    @pl.when(me > 0)
+    def _():
+        halo_copy().wait_recv()
+        halo[...] = halo_in[...].astype(F32)
+
+    relay_lag, near_lag = min(RELAY_LAG, steps), min(NEAR_LAG, steps)
+
+    def step(g, carry):
+        states(g)
+
+        @pl.when(me == 0)
+        def _():
+            begin(g, 0, True, True)
+
+        @pl.when(me == n - 1)
+        def _():
+            for q in range(G):
+                log_out[g * G + q] = log_own[g * G + q]
+            log_copy(g).start()
+            begin(g, n - 1, False, True)
+
+        @pl.when(g >= near_lag)
+        def _():
+            @pl.when(me == 0)
+            def _():
+                begin(g - near_lag, 0, True, False)
+
+            @pl.when(me == n - 1)
+            def _():
+                begin(g - near_lag, n - 1, False, False)
+
+        @pl.when(g + lead_steps < steps)
+        def _():
+            project(g + lead_steps)
+
+        if n > 2:
+
+            @pl.when((g == min(1, steps - 1)) & (me > 0) & (me < n - 1))
+            def _():
+                newest_copy().wait_recv()
+                newest_copy().start()
+
+        @pl.when(g >= relay_lag)
+        def _():
+            relay(g - relay_lag)
+
         return carry
 
     lax.fori_loop(0, steps, step, 0)
-
-    logs[me] = logs_out[...]
-    recv[me] = sendbuf[me]
-
-    RH = heads * R
-    head_rows = ones_where((RH, HEADS), lambda l, i: i == lead + lax.div(l, R))
+    for g in range(steps - near_lag, steps):
+
+        @pl.when(me == 0)
+        def _(g=g):
+            begin(g, 0, True, False)
+
+        @pl.when(me == n - 1)
+        def _(g=g):
+            begin(g, n - 1, False, False)
+
     head_cols = ones_where((HEADS, RH), lambda i, l: i == lead + lax.div(l, R))
+    local_cols = ones_where((128, RH), lambda i, l: i == lax.div(l, R))
+    local = ones_where((HEADS, 128), lambda i, c: (i == lead + c) & (c < heads))
     pick = ones_where(
         (F, RH), lambda c, l: c == lax.div(l, R) * P_SIZE + me * R + lax.rem(l, R), BF16
     )
@@ -456,44 +588,70 @@
     gate_here = silu(jnp.dot(gate, pick, preferred_element_type=F32))
     gain_here = jnp.sum(exact_dot(gain_ref[...], row_pick) * head_cols, axis=0, keepdims=True)
     skip_here = exact_dot(skip_ref[...], head_cols)
-    new_dt = softplus(new_step + bias)
-    dt_here = exact_dot(new_dt, head_cols)
-    keep_here = jnp.exp(-exact_dot(speed * new_dt, head_cols))
-
-    @pl.when(me < n - 1)
+    new_dt = softplus(new_step + exact_dot(bias, local))
+    dt_here = exact_dot(new_dt, local_cols)
+    keep_here = jnp.exp(-exact_dot(exact_dot(speed, local) * new_dt, local_cols))
+
+    @pl.when(me == 0)
     def _():
-        pltpu.make_async_remote_copy(
-            newest, newest, new_send.at[0], new_recv, device_id=at(1), device_id_type=MESH
-        ).wait_recv()
-
-    new_mixed = silu(newest[0] + new_raw * taps[CONV - 1 : CONV, :]).astype(BF16)
+        newest_copy().wait_recv()
+
+    new_mixed = silu(newest[...] + new_raw * taps[CONV - 1 : CONV, :]).astype(BF16)
     new_input = jnp.dot(new_mixed[:, 0:F], pick, preferred_element_type=F32)
     new_in = new_mixed[:, F:C].astype(F32)
     new_out = new_mixed[:, C : C + STATE]
     both = jnp.sum(new_in * new_out.astype(F32), axis=1, keepdims=True)
-
     where_row = lax.broadcasted_iota(jnp.int32, (SP, RH), 0)
-    y = jnp.zeros((SP, RH), F32)
-    for g in range(steps):
-        for k in range(1, n):
-            log_copy(g, k).wait_recv()
-            state_copy(g, k).wait_recv()
-        for p in range(g * G, (g + 1) * G):
-            later = jnp.zeros((1, HEADS), F32)
-            tot = jnp.zeros((RH, STATE), F32)
-            for s in reversed(range(n)):
-                factor = jnp.sum(head_rows * jnp.exp(later), axis=1, keepdims=True)
-                tot = tot + factor * recv[s, p].astype(F32)
-                later = later + logs[s, p, 0:1, 0:HEADS]
-            kept = tot.astype(BF16)
-            cache_ref[p] = kept
+
+    def out_copy(g):
+        here = pl.ds(g * G, G)
+        return pltpu.make_async_copy(kept_buf.at[here], cache_hbm.at[here], out_sem.at[g])
+
+    def finish(g, y):
+        for s in range(n):
+
+            @pl.when(me == s)
+            def _(s=s):
+                if s > 0:
+                    flow(g, s - 1, True, False).wait_recv()
+                if s == 0:
+                    log_copy(g).wait_recv()
+                if s < n - 1:
+                    flow(g, s + 1, False, False).wait_recv()
+
+        for q in range(G):
+            p = g * G + q
+            before, after = decay[p], later_factor(p)
+            kept = []
+            for h in range(heads):
+                z = (p, me, slice(h * R, (h + 1) * R))
+                t = own[z].astype(F32) + from_left[z].astype(F32) * before[h : h + 1, :]
+                t = t * after[h : h + 1, :] + from_right[z].astype(F32)
+                kept.append(t.astype(BF16))
+            kept = jnp.concatenate(kept, axis=0)
+            kept_buf[p] = kept
             part = lax.dot_general(
                 new_out, kept, (((1,), (1,)), ((), ())), preferred_element_type=F32
             )
             y = jnp.where(where_row == p, part, y)
+        out_copy(g).start()
+        return y
+
+    y = jnp.zeros((SP, RH), F32)
+    left = list(range(steps - relay_lag, steps))
+    done = 0
+    for i, g in enumerate(left):
+        relay(g)
+        upto = max(done, g - 2) if i + 1 < len(left) else steps
+        if upto > done:
+            y = lax.fori_loop(done, upto, finish, y)
+            done = upto
+
     readout = keep_here * y + dt_here * new_input * both + skip_here * new_input
     gated = readout * gate_here
-    sq = jnp.broadcast_to(jnp.sum(gated * gated, axis=1, keepdims=True), sq_out.shape)
+    square_sum = jnp.broadcast_to(jnp.sum(gated * gated, axis=1, keepdims=True), (SP, 128))
+    diagonal = ones_where((SP, 128), lambda i, c: i == c)
+    sq = jnp.sum(square_sum * diagonal, axis=0, keepdims=True)
     sq_out[...] = sq
 
     def sq_copy(i):
@@ -504,27 +662,41 @@
 
     for i in range(len(peers)):
         sq_copy(i).start()
+    for g in range(steps):
+        out_copy(g).wait()
+    for s in range(n):
+
+        @pl.when(me == s)
+        def _(s=s):
+            for g in range(steps):
+                for right in (False, True):
+                    for far in (False, True):
+                        c = flow(g, s, right, far)
+                        if c is not None:
+                            c.wait_send()
+                if s > 0:
+                    log_copy(g).wait_send()
+
+    @pl.when(me < n - 1)
+    def _():
+        halo_copy().wait_send()
+
+    @pl.when(me > 0)
+    def _():
+        newest_copy().wait_send()
+
     for i in range(len(peers)):
         sq_copy(i).wait_recv()
         sq = sq + sq_in[i]
-    scale = lax.rsqrt(sq[:, 0:1] / (HEADS * P_SIZE) + epsilon)
+    mean = jnp.sum(diagonal * sq, axis=1, keepdims=True) / (HEADS * P_SIZE)
+    scale = lax.rsqrt(mean + epsilon)
     read_ref[...] = (gated * scale * gain_here).astype(BF16)[0:S]
 
     for i in range(len(peers)):
         sq_copy(i).wait_send()
-    for k in range(1, n):
-        for g in range(steps):
-            log_copy(g, k).wait_send()
-            state_copy(g, k).wait_send()
-
-    @pl.when(me < n - 1)
-    def _():
-        halo_copy().wait_send()
-
-    @pl.when(me == n - 1)
-    def _():
-        for k in range(1, n):
-            newest_copy(k).wait_send()
+
+
+LEAD, RELAY_LAG, NEAR_LAG = 2, 2, 2
 
 
 def fused(*args):
@@ -536,6 +708,7 @@
     R = P_SIZE // n
     G = next(g for g in (2, 3, 1) if S % g == 0)
     steps = S // G
+    slots = min(LEAD, steps)
     C, RH, SP = F + STATE, heads * R, 16
     dims = (n, m, S, L, heads, R, G)
     flat = list(args)
@@ -553,37 +726,43 @@
             jax.ShapeDtypeStruct((S, RH), BF16),
         ),
         in_specs=specs,
-        out_specs=(vmem, vmem),
+        out_specs=(pl.BlockSpec(memory_space=pltpu.HBM), vmem),
         scratch_shapes=[
             pltpu.VMEM((S, L, D), BF16),
             pltpu.VMEM((S + 1, 16, D), BF16),
             pltpu.VMEM((D, C + STATE), BF16),
             pltpu.VMEM((D, STATE), BF16),
-            pltpu.VMEM((HEADS, D), BF16),
+            pltpu.VMEM((heads, D), BF16),
             pltpu.VMEM((D, F), BF16),
-            pltpu.VMEM((S, HEADS, L), F32),
+            pltpu.VMEM((S, heads, L), F32),
             pltpu.VMEM((CONV, C + STATE), F32),
-            pltpu.VMEM((G, 8 + L, C), F32),
+            pltpu.VMEM((slots, G, 8 + L, C), F32),
+            pltpu.VMEM((slots, G, 2 * heads, L), BF16),
             pltpu.VMEM((CONV - 1, SP, C), BF16),
             pltpu.VMEM((CONV - 1, SP, C), BF16),
             pltpu.VMEM((CONV - 1, SP, C), F32),
-            pltpu.VMEM((1, SP, C + STATE), F32),
-            pltpu.VMEM((S, 8, 128), F32),
-            pltpu.VMEM((n, S, 8, 128), F32),
-            pltpu.VMEM((n, S, RH, STATE), BF16),
-            pltpu.VMEM((n, S, RH, STATE), BF16),
-            pltpu.VMEM((SP, 128), F32),
-            pltpu.VMEM((n * m - 1, SP, 128), F32),
-            pltpu.VMEM((2 * HEADS, F), BF16),
+            pltpu.VMEM((SP, C + STATE), F32),
+            pltpu.VMEM((2, HEADS, 128), F32),
+            pltpu.VMEM((S, heads, 128), F32),
+            pltpu.VMEM((S, 1, 128), F32),
+            pltpu.VMEM((S, 1, 128), F32),
+            pltpu.VMEM((S, 1, 128), F32),
+            pltpu.VMEM((S, n, RH, STATE), BF16),
+            pltpu.VMEM((S, n, RH, STATE), BF16),
+            pltpu.VMEM((S, n, RH, STATE), BF16),
+            pltpu.VMEM((S, RH, STATE), BF16),
+            pltpu.VMEM((1, 128), F32),
+            pltpu.VMEM((n * m - 1, 1, 128), F32),
+            pltpu.VMEM((2 * heads, F), BF16),
             dma((7,)),
             dma((steps,)),
             dma((2,)),
-            dma((n,)),
-            dma,
-            dma((steps, n)),
-            dma((steps, n)),
-            dma((steps, n)),
-            dma((steps, n)),
+            dma((2,)),
+            dma((4, steps)),
+            dma((4, steps)),
+            dma((steps,)),
+            dma((steps,)),
+            dma((steps,)),
             dma((n * m,)),
             dma((n * m,)),
         ],
@@ -600,6 +779,7 @@
     return (
         n > 1
         and F % 128 == 0
+        and heads % 8 == 0
         and R % 16 == 0
         and (heads * R) % 128 == 0
         and S <= 16

time: 62.2 us -> 80.8 us (1.30)
  Pallas kernels: 58.1 us -> 76.8 us
    pallas_call x1, Pallas kernels: 58.1 us -> 76.8 us  [fused(): pl.pallas_call(lambda *refs: mixer_kernel(dims, *refs), out_shape=(jax.Sh...]
where the time goes in v1:
time: 80.8 us; the launch traced here: 80.6 us
  Pallas kernels  76.8 us (95%)
  local copies, waits for them, and re-layouts  3.14 us (4%)
    pallas_call x1, Pallas kernels, fused(): pl.pallas_call(lambda *refs: mixer_kernel(dims, *refs), out_shape=(jax.Sh...  76.8 us
    unnamed x1, local copies, waits for them, and re-layouts  1.77 us

profile of v1, /device:TPU:0, one launch (start us, length us, event | category | flops | bytes accessed | tf_op | source)
XLA Modules:
  0.0 80.6 jit_solution(2882792033636863504)
XLA Ops:
  0.6 76.8 %shard_map.158 = (bf16[12,128,128]{2,1,0:T(8,128)(2,1)}, bf16[12,128]{1,0:T(8,128)(2,1)}) custom-call(bf16[12,128,2048]{2,1,0:T(8,128)(2,1)} %refs_0_.1, bf16[12,2048]{1,0:T(8,128)(2,1)} %refs_1_.1, bf16[2048,512]{1,0:T(8,128)(2,1)} %refs_2_.1, bf16[2048,512]{1,0:T(8,128)(2,1)} %refs_3_.1, bf16[2048,256]{1,0:T(8,128)(2,1)} %refs_4_.1, ...), custom_call_target="tpu_custom_call" | custom-call | tf_op jit(solution)/shard_map/pallas_call | solution.py:722
  77.4 1.4 %reshape.23 = bf16[12,8,16]{2,1,0:T(8,128)(2,1)} reshape(bf16[12,128]{1,0:T(8,128)(2,1)} %get-tuple-element.5) | data formatting | bytes 6144 | tf_op jit(solution)/shard_map/reshape | solution.py:773
  78.8 1.8 %copy.18 = bf16[12,8,16,128]{3,2,1,0:T(8,128)(2,1)} copy(bf16[12,8,16,128]{3,2,1,0:T(8,128)(2,1)} %bitcast.6) | data formatting | bytes 786432

commit v2 on v1

--- a/solution.py
+++ b/solution.py
@@ -214,12 +214,11 @@
     skip_ref,
     gain_ref,
     off_hbm,
-    cache_hbm,
+    cache_ref,
     read_ref,
     xbuf,
     edge,
     wall,
-    wq,
     ws,
     wg,
     off,
@@ -228,7 +227,6 @@
     wsplit,
     halo_out,
     halo_in,
-    halo,
     newest,
     heads_t,
     decay,
@@ -238,7 +236,6 @@
     own,
     from_left,
     from_right,
-    kept_buf,
     sq_out,
     sq_in,
     expand,
@@ -250,7 +247,6 @@
     st_recv,
     log_send,
     log_recv,
-    out_sem,
     sq_send,
     sq_recv,
 ):
@@ -277,33 +273,28 @@
             x_hbm.at[pl.ds(g * G, G)], xbuf.at[pl.ds(g * G, G)], x_sem.at[g]
         )
 
+    peers = [(a, b) for a in range(n) for b in range(m) if (a, b) != (0, 0)]
+
+    def at(a, b=0):
+        return {"sp": lax.rem(me + a, n), "tp": lax.rem(tp + b, m)}
+
+    barrier = pltpu.get_barrier_semaphore()
+    for a, b in peers:
+        pl.semaphore_signal(barrier, inc=1, device_id=at(a, b), device_id_type=MESH)
+
     first = [
         load(ws_hbm.at[pl.ds(lead, heads), :], ws, 0),
         load(x_hbm.at[:, pl.ds(L - 16, 16)], edge.at[pl.ds(0, S)], 1),
-        load(wk_hbm.at[:, pl.ds(gcol, STATE)], wall.at[:, pl.ds(F, STATE)], 2),
-        load(wv_hbm, wall.at[:, pl.ds(0, F)], 3),
-        load(wq_hbm.at[:, pl.ds(gcol, STATE)], wq, 4),
+        load(wk_hbm.at[:, pl.ds(gcol, STATE)], wall.at[:, pl.ds(128 + F, STATE)], 2),
+        load(wq_hbm.at[:, pl.ds(gcol, STATE)], wall.at[:, pl.ds(128 + C, STATE)], 3),
+        load(wv_hbm, wall.at[:, pl.ds(128, F)], 4),
     ]
-    off_load = load(off_hbm.at[:, pl.ds(lead, heads), :], off, 5)
-    for g in range(steps):
-        load_x(g).start()
-    gate_load = load(wg_hbm, wg, 6)
-
-    peers = [(a, b) for a in range(n) for b in range(m) if (a, b) != (0, 0)]
-
-    def at(a, b=0):
-        return {"sp": lax.rem(me + a, n), "tp": lax.rem(tp + b, m)}
-
-    barrier = pltpu.get_barrier_semaphore()
-    for a, b in peers:
-        pl.semaphore_signal(barrier, inc=1, device_id=at(a, b), device_id_type=MESH)
 
     taps[:, 0:F] = tv_ref[:, pl.ds(fcol, F)].astype(F32)
     taps[:, F:C] = tk_ref[:, pl.ds(gcol, STATE)].astype(F32)
     taps[:, C : C + STATE] = tq_ref[:, pl.ds(gcol, STATE)].astype(F32)
     edge[S] = jnp.zeros(edge.shape[1:], BF16)
     edge[S, 0:S, :] = next_ref[...]
-    halo_out[...] = jnp.zeros_like(halo_out)
     head_of = ones_where((heads, F), lambda i, c: i == lax.div(c, P_SIZE))
     expand[...] = jnp.concatenate([head_of, head_of], axis=0).astype(BF16)
     bias = bias_ref[...]
@@ -329,34 +320,49 @@
     eye = ones_where((heads, 128), lambda i, c: i == c)
     later_ones = ones_where((L, L), lambda u, t: u > t, BF16)
 
-    first[0].wait()
-    wall[:, C : C + STATE] = jnp.concatenate(
-        [ws[...], jnp.zeros((STATE - heads, ws.shape[1]), BF16)], axis=0
-    ).T
     for c in first[1:4]:
         c.wait()
+    load_x(0).start()
+    first[4].wait()
+    off_load = load(off_hbm.at[:, pl.ds(lead, heads), :], off, 5)
     rows = edge[...].reshape((S + 1) * 16, edge.shape[2])
-    eproj = jnp.dot(rows, wall[...], preferred_element_type=F32).astype(BF16).astype(F32)
+    eproj = jnp.dot(rows, wall[:, 128:], preferred_element_type=F32).astype(BF16).astype(F32)
     e3 = eproj.reshape(S + 1, 16, C + STATE)
-    for j in range(CONV - 1):
-        halo_out[j, 0:S, :] = e3[0:S, 16 - (CONV - 1) + j, 0:C].astype(BF16)
-
+    new_raw = e3[S]
+    tail_rows = halo_out.shape[1] - G * (CONV - 1)
+    for g in range(steps):
+        tails = [e3[g * G + q, 16 - (CONV - 1) :, 0:C] for q in range(G)]
+        if tail_rows:
+            tails.append(jnp.zeros((tail_rows, C), F32))
+        halo_out[g] = jnp.concatenate(tails, axis=0).astype(BF16)
+
+    for g in range(1, steps):
+        load_x(g).start()
+    gate_load = load(wg_hbm, wg, 6)
     pl.semaphore_wait(barrier, len(peers))
 
-    def halo_copy():
+    def halo_copy(k):
+        here = pl.ds(0, 1) if k == 0 else pl.ds(1, steps - 1)
         return pltpu.make_async_remote_copy(
-            halo_out, halo_in, halo_sem.at[0], halo_sem.at[1], device_id=at(1), device_id_type=MESH
+            halo_out.at[here],
+            halo_in.at[here],
+            halo_sem.at[0, k],
+            halo_sem.at[1, k],
+            device_id=at(1),
+            device_id_type=MESH,
         )
 
+    halo_parts = range(2 if steps > 1 else 1)
+
     @pl.when(me < n - 1)
     def _():
-        halo_copy().start()
-
-    first[4].wait()
-    eq = jnp.dot(rows, wq[...], preferred_element_type=F32).astype(BF16).astype(F32)
-    q3 = eq.reshape(S + 1, 16, STATE)
-    new_raw = jnp.concatenate([e3[S, :, 0:C], q3[S]], axis=1)
-    new_step = e3[S, :, C : C + STATE]
+        for k in halo_parts:
+            halo_copy(k).start()
+
+    first[0].wait()
+    wall[:, 0:128] = jnp.concatenate(
+        [ws[...], jnp.zeros((128 - heads, ws.shape[1]), BF16)], axis=0
+    ).T
 
     def newest_copy():
         return pltpu.make_async_remote_copy(
@@ -368,49 +374,37 @@
             device_id_type=MESH,
         )
 
-    @pl.when(me == n - 1)
-    def _():
-        total = jnp.zeros((S, C + STATE), F32)
-        for j in range(CONV - 1):
-            row = 16 - (CONV - 1) + j
-            tail = jnp.concatenate([e3[0:S, row, 0:C], q3[0:S, row, :]], axis=1)
-            total = total + tail * taps[j : j + 1, :]
-        newest[...] = jnp.zeros_like(newest)
-        newest[0:S, :] = total
-        newest_copy().start()
-
     def span(s, right, far):
         if right:
             return (s + 2, n) if far else (s + 1, s + 2)
         return (0, s - 1) if far else (s - 1, s)
 
-    def flow(g, s, right, far):
+    def flow(p, s, right, far):
         lo, hi = span(s, right, far)
         if not (0 <= lo < hi <= n):
             return None
         k = 2 * int(right) + int(far)
-        here = (pl.ds(g * G, G), pl.ds(lo, hi - lo))
+        here = (p, pl.ds(lo, hi - lo))
         return pltpu.make_async_remote_copy(
             own.at[here],
             (from_left if right else from_right).at[here],
-            st_send.at[k, g],
-            st_recv.at[k, g],
+            st_send.at[k, p],
+            st_recv.at[k, p],
             device_id=at(1 if right else n - 1),
             device_id_type=MESH,
         )
 
-    def begin(g, s, right, far):
-        c = flow(g, s, right, far)
+    def begin(p, s, right, far):
+        c = flow(p, s, right, far)
         if c is not None:
             c.start()
 
-    def log_copy(g):
-        here = pl.ds(g * G, G)
+    def log_copy(p):
         return pltpu.make_async_remote_copy(
-            log_out.at[here],
-            log_in.at[here],
-            log_send.at[g],
-            log_recv.at[g],
+            log_out.at[p],
+            log_in.at[p],
+            log_send.at[p],
+            log_recv.at[p],
             device_id=at(n - 1),
             device_id_type=MESH,
         )
@@ -419,12 +413,12 @@
         load_x(g).wait()
         slot = lax.rem(g, lead_steps)
         xg = xbuf[pl.ds(g * G, G)].reshape(G * L, xbuf.shape[2])
-        acc = jnp.dot(xg, wall[...], preferred_element_type=F32).astype(BF16).astype(F32)
+        acc = jnp.dot(xg, wall[:, 0 : 128 + C], preferred_element_type=F32).astype(BF16).astype(F32)
         for q in range(G):
             p = g * G + q
             raw = acc[q * L : (q + 1) * L]
-            pad[slot, q, 8 : 8 + L, :] = raw[:, 0:C]
-            dt = softplus(raw[:, C : C + STATE].T[0:heads] + bias_t)
+            pad[slot, q, 8 : 8 + L, :] = raw[:, 128:]
+            dt = softplus(raw[:, 0:128].T[0:heads] + bias_t)
             ld = off[p] - speed_t * dt
             a = ld.astype(BF16).astype(F32)
             b = (ld - a).astype(BF16).astype(F32)
@@ -438,13 +432,40 @@
             hi = w.astype(BF16).astype(F32)
             wsplit[slot, q] = jnp.concatenate([hi, w - hi], axis=0).astype(BF16)
 
+    depth, behind = min(DEPTH, S), min(BEHIND, S)
+
+    def feed(p, s, right):
+        if flow(0, s, right, True) is not None:
+
+            @pl.when((p >= depth) & (p < S + depth))
+            def _():
+                flow(p - depth, s, right, True).wait_send()
+
+            @pl.when(p < S)
+            def _():
+                begin(p, s, right, True)
+
+        @pl.when(p >= depth + behind)
+        def _():
+            flow(p - depth - behind, s, right, False).wait_send()
+
+        @pl.when(p >= behind)
+        def _():
+            begin(p - behind, s, right, False)
+
+    def feed_rest(s, right):
+        def one(p, carry):
+            feed(p, s, right)
+            return carry
+
+        lax.fori_loop(S, S + behind, one, 0)
+
     def states(g):
         slot = lax.rem(g, lead_steps)
+        before = halo_in[g].astype(F32)
         for q in range(G):
             p = g * G + q
-            for j in range(CONV - 1):
-                r = 8 - (CONV - 1) + j
-                pad[slot, q, r : r + 1, :] = halo[j, pl.ds(p, 1), :]
+            pad[slot, q, 8 - (CONV - 1) : 8, :] = before[q * (CONV - 1) : (q + 1) * (CONV - 1)]
             wide = lax.dot_general(
                 wsplit[slot, q],
                 expand[...],
@@ -472,81 +493,86 @@
                         b = hh * P_SIZE + d * R
                         own[p, d, h * R : (h + 1) * R, :] = share[b : b + R]
 
+            @pl.when(me == 0)
+            def _(p=p):
+                feed(p, 0, True)
+
+            @pl.when(me == n - 1)
+            def _(p=p):
+                log_out[p] = log_own[p]
+                log_copy(p).start()
+                feed(p, n - 1, False)
+
     def later_factor(p):
         row = jnp.sum(eye * log_in[p], axis=1, keepdims=True)
         return jnp.exp(jnp.broadcast_to(row, (heads, 128)))
 
-    def relay(g):
+    def sum_right(p, s):
+        flow(p, s - 1, True, True).wait_recv()
+        factor = decay[p]
+        for d in reversed(range(s + 1, n)):
+            for h in range(heads):
+                z = (p, d, slice(h * R, (h + 1) * R))
+                got = from_left[z].astype(F32) * factor[h : h + 1, :]
+                own[z] = (own[z].astype(F32) + got).astype(BF16)
+        begin(p, s, True, True)
+        begin(p, s, True, False)
+
+    def sum_left(p, s):
+        log_copy(p).wait_recv()
+        log_out[p] = log_in[p] + log_own[p]
+        log_copy(p).start()
+        flow(p, s + 1, False, True).wait_recv()
+        factor = later_factor(p)
+        for d in range(s):
+            for h in range(heads):
+                z = (p, d, slice(h * R, (h + 1) * R))
+                mine = own[z].astype(F32) * factor[h : h + 1, :]
+                own[z] = (from_right[z].astype(F32) + mine).astype(BF16)
+        begin(p, s, False, True)
+        begin(p, s, False, False)
+
+    def relay(g, outer):
         for s in range(1, n - 1):
 
             @pl.when(me == s)
             def _(s=s):
-                if s + 1 < n:
-                    flow(g, s - 1, True, True).wait_recv()
                 for q in range(G):
-                    p = g * G + q
-                    factor = decay[p]
-                    for d in range(s + 1, n):
-                        for h in range(heads):
-                            z = (p, d, slice(h * R, (h + 1) * R))
-                            got = from_left[z].astype(F32) * factor[h : h + 1, :]
-                            own[z] = (own[z].astype(F32) + got).astype(BF16)
-                begin(g, s, True, True)
-                begin(g, s, True, False)
-                log_copy(g).wait_recv()
-                for q in range(G):
-                    p = g * G + q
-                    log_out[p] = log_in[p] + log_own[p]
-                log_copy(g).start()
-                flow(g, s + 1, False, True).wait_recv()
-                for q in range(G):
-                    p = g * G + q
-                    factor = later_factor(p)
-                    for d in range(s):
-                        for h in range(heads):
-                            z = (p, d, slice(h * R, (h + 1) * R))
-                            mine = own[z].astype(F32) * factor[h : h + 1, :]
-                            own[z] = (from_right[z].astype(F32) + mine).astype(BF16)
-                begin(g, s, False, True)
-                begin(g, s, False, False)
+                    if outer == (s < n - 1 - s):
+                        sum_right(g * G + q, s)
+                    else:
+                        sum_left(g * G + q, s)
 
     off_load.wait()
     lax.fori_loop(0, lead_steps, lambda g, carry: (project(g), carry)[1], 0)
+    @pl.when(me == n - 1)
+    def _():
+        total = jnp.zeros((S, C + STATE), F32)
+        for j in range(CONV - 1):
+            row = 16 - (CONV - 1) + j
+            total = total + e3[0:S, row, :] * taps[j : j + 1, :]
+        newest[...] = jnp.zeros_like(newest)
+        newest[0:S, :] = total
+        newest_copy().start()
 
     @pl.when(me == 0)
     def _():
-        halo[...] = jnp.zeros_like(halo)
+        halo_in[...] = jnp.zeros_like(halo_in)
 
     @pl.when(me > 0)
     def _():
-        halo_copy().wait_recv()
-        halo[...] = halo_in[...].astype(F32)
-
-    relay_lag, near_lag = min(RELAY_LAG, steps), min(NEAR_LAG, steps)
+        halo_copy(0).wait_recv()
+
+    relay_lag = min(RELAY_LAG, steps)
 
     def step(g, carry):
+        if steps > 1:
+
+            @pl.when((g == 1) & (me > 0))
+            def _():
+                halo_copy(1).wait_recv()
+
         states(g)
-
-        @pl.when(me == 0)
-        def _():
-            begin(g, 0, True, True)
-
-        @pl.when(me == n - 1)
-        def _():
-            for q in range(G):
-                log_out[g * G + q] = log_own[g * G + q]
-            log_copy(g).start()
-            begin(g, n - 1, False, True)
-
-        @pl.when(g >= near_lag)
-        def _():
-            @pl.when(me == 0)
-            def _():
-                begin(g - near_lag, 0, True, False)
-
-            @pl.when(me == n - 1)
-            def _():
-                begin(g - near_lag, n - 1, False, False)
 
         @pl.when(g + lead_steps < steps)
         def _():
@@ -554,28 +580,24 @@
 
         if n > 2:
 
-            @pl.when((g == min(1, steps - 1)) & (me > 0) & (me < n - 1))
-            def _():
-                newest_copy().wait_recv()
-                newest_copy().start()
+            for s in range(1, n - 1):
+
+                @pl.when((g == min(FORWARD_AT * (n - 1 - s), steps - 1)) & (me == s))
+                def _():
+                    newest_copy().wait_recv()
+                    newest_copy().start()
 
         @pl.when(g >= relay_lag)
         def _():
-            relay(g - relay_lag)
+            relay(g - relay_lag, True)
+
+        @pl.when(g >= relay_lag + 1)
+        def _():
+            relay(g - relay_lag - 1, False)
 
         return carry
 
     lax.fori_loop(0, steps, step, 0)
-    for g in range(steps - near_lag, steps):
-
-        @pl.when(me == 0)
-        def _(g=g):
-            begin(g, 0, True, False)
-
-        @pl.when(me == n - 1)
-        def _(g=g):
-            begin(g, n - 1, False, False)
-
     head_cols = ones_where((HEADS, RH), lambda i, l: i == lead + lax.div(l, R))
     local_cols = ones_where((128, RH), lambda i, l: i == lax.div(l, R))
     local = ones_where((HEADS, 128), lambda i, c: (i == lead + c) & (c < heads))
@@ -588,7 +610,8 @@
     gate_here = silu(jnp.dot(gate, pick, preferred_element_type=F32))
     gain_here = jnp.sum(exact_dot(gain_ref[...], row_pick) * head_cols, axis=0, keepdims=True)
     skip_here = exact_dot(skip_ref[...], head_cols)
-    new_dt = softplus(new_step + exact_dot(bias, local))
+    new_step = jnp.dot(edge[S], wall[:, 0:128], preferred_element_type=F32).astype(BF16)
+    new_dt = softplus(new_step.astype(F32) + exact_dot(bias, local))
     dt_here = exact_dot(new_dt, local_cols)
     keep_here = jnp.exp(-exact_dot(exact_dot(speed, local) * new_dt, local_cols))
 
@@ -603,21 +626,27 @@
     both = jnp.sum(new_in * new_out.astype(F32), axis=1, keepdims=True)
     where_row = lax.broadcasted_iota(jnp.int32, (SP, RH), 0)
 
-    def out_copy(g):
-        here = pl.ds(g * G, G)
-        return pltpu.make_async_copy(kept_buf.at[here], cache_hbm.at[here], out_sem.at[g])
+    @pl.when(me == 0)
+    def _():
+        feed_rest(0, True)
+
+    @pl.when(me == n - 1)
+    def _():
+        feed_rest(n - 1, False)
 
     def finish(g, y):
         for s in range(n):
 
             @pl.when(me == s)
             def _(s=s):
-                if s > 0:
-                    flow(g, s - 1, True, False).wait_recv()
-                if s == 0:
-                    log_copy(g).wait_recv()
-                if s < n - 1:
-                    flow(g, s + 1, False, False).wait_recv()
+                for q in range(G):
+                    p = g * G + q
+                    if s > 0:
+                        flow(p, s - 1, True, False).wait_recv()
+                    if s == 0:
+                        log_copy(p).wait_recv()
+                    if s < n - 1:
+                        flow(p, s + 1, False, False).wait_recv()
 
         for q in range(G):
             p = g * G + q
@@ -629,23 +658,19 @@
                 t = t * after[h : h + 1, :] + from_right[z].astype(F32)
                 kept.append(t.astype(BF16))
             kept = jnp.concatenate(kept, axis=0)
-            kept_buf[p] = kept
+            cache_ref[p] = kept
             part = lax.dot_general(
                 new_out, kept, (((1,), (1,)), ((), ())), preferred_element_type=F32
             )
             y = jnp.where(where_row == p, part, y)
-        out_copy(g).start()
         return y
 
-    y = jnp.zeros((SP, RH), F32)
-    left = list(range(steps - relay_lag, steps))
-    done = 0
-    for i, g in enumerate(left):
-        relay(g)
-        upto = max(done, g - 2) if i + 1 < len(left) else steps
-        if upto > done:
-            y = lax.fori_loop(done, upto, finish, y)
-            done = upto
+    for g in range(steps - relay_lag, steps):
+        relay(g, True)
+        if g > 0:
+            relay(g - 1, False)
+    relay(steps - 1, False)
+    y = lax.fori_loop(0, steps, finish, jnp.zeros((SP, RH), F32))
 
     readout = keep_here * y + dt_here * new_input * both + skip_here * new_input
     gated = readout * gate_here
@@ -662,24 +687,34 @@
 
     for i in range(len(peers)):
         sq_copy(i).start()
-    for g in range(steps):
-        out_copy(g).wait()
     for s in range(n):
 
         @pl.when(me == s)
         def _(s=s):
-            for g in range(steps):
+            end = s in (0, n - 1)
+
+            def sent(p, carry):
                 for right in (False, True):
                     for far in (False, True):
-                        c = flow(g, s, right, far)
-                        if c is not None:
+                        c = flow(p, s, right, far)
+                        if c is None:
+                            continue
+                        fed = p < S + min(0, behind - depth) if far else p < S - depth
+
+                        @pl.when(jnp.logical_not(fed & end))
+                        def _(c=c):
                             c.wait_send()
+
                 if s > 0:
-                    log_copy(g).wait_send()
+                    log_copy(p).wait_send()
+                return carry
+
+            lax.fori_loop(0, S, sent, 0)
 
     @pl.when(me < n - 1)
     def _():
-        halo_copy().wait_send()
+        for k in halo_parts:
+            halo_copy(k).wait_send()
 
     @pl.when(me > 0)
     def _():
@@ -696,7 +731,26 @@
         sq_copy(i).wait_send()
 
 
-LEAD, RELAY_LAG, NEAR_LAG = 2, 2, 2
+def on_chip(array):
+    return pltpu.with_memory_space_constraint(array, pltpu.VMEM)
+
+
+def emit_kernel(dims, cache_ref, read_ref, cache_hbm, out_ref, sem):
+    heads, R = dims
+    S, RH = read_ref.shape
+    copy = pltpu.make_async_copy(cache_ref, cache_hbm, sem)
+    copy.start()
+    spread = ones_where((heads, RH), lambda h, l: h == lax.div(l, R))
+    pick = ones_where((RH, R), lambda l, r: lax.rem(l, R) == r, BF16)
+    value = read_ref[...].astype(F32)
+    rows = jnp.concatenate([value[p : p + 1] * spread for p in range(S)], axis=0).astype(BF16)
+    out = jnp.dot(rows, pick, preferred_element_type=F32)
+    out_ref[...] = out.reshape(S, heads, R).astype(BF16)
+    copy.wait()
+
+
+LEAD, RELAY_LAG, FORWARD_AT = 1, 1, 2
+DEPTH, BEHIND = 4, 8
 
 
 def fused(*args):
@@ -709,6 +763,7 @@
     G = next(g for g in (2, 3, 1) if S % g == 0)
     steps = S // G
     slots = min(LEAD, steps)
+    halo_rows = -(-G * (CONV - 1) // 8) * 8
     C, RH, SP = F + STATE, heads * R, 16
     dims = (n, m, S, L, heads, R, G)
     flat = list(args)
@@ -722,25 +777,23 @@
     cache, read = pl.pallas_call(
         lambda *refs: mixer_kernel(dims, *refs),
         out_shape=(
-            jax.ShapeDtypeStruct((S, RH, STATE), BF16),
-            jax.ShapeDtypeStruct((S, RH), BF16),
+            pltpu.VMEM((S, RH, STATE), BF16),
+            pltpu.VMEM((S, RH), BF16),
         ),
         in_specs=specs,
-        out_specs=(pl.BlockSpec(memory_space=pltpu.HBM), vmem),
+        out_specs=(vmem, vmem),
         scratch_shapes=[
             pltpu.VMEM((S, L, D), BF16),
             pltpu.VMEM((S + 1, 16, D), BF16),
-            pltpu.VMEM((D, C + STATE), BF16),
-            pltpu.VMEM((D, STATE), BF16),
+            pltpu.VMEM((D, 128 + C + STATE), BF16),
             pltpu.VMEM((heads, D), BF16),
             pltpu.VMEM((D, F), BF16),
             pltpu.VMEM((S, heads, L), F32),
             pltpu.VMEM((CONV, C + STATE), F32),
             pltpu.VMEM((slots, G, 8 + L, C), F32),
             pltpu.VMEM((slots, G, 2 * heads, L), BF16),
-            pltpu.VMEM((CONV - 1, SP, C), BF16),
-            pltpu.VMEM((CONV - 1, SP, C), BF16),
-            pltpu.VMEM((CONV - 1, SP, C), F32),
+            pltpu.VMEM((steps, halo_rows, C), BF16),
+            pltpu.VMEM((steps, halo_rows, C), BF16),
             pltpu.VMEM((SP, C + STATE), F32),
             pltpu.VMEM((2, HEADS, 128), F32),
             pltpu.VMEM((S, heads, 128), F32),
@@ -750,19 +803,17 @@
             pltpu.VMEM((S, n, RH, STATE), BF16),
             pltpu.VMEM((S, n, RH, STATE), BF16),
             pltpu.VMEM((S, n, RH, STATE), BF16),
-            pltpu.VMEM((S, RH, STATE), BF16),
             pltpu.VMEM((1, 128), F32),
             pltpu.VMEM((n * m - 1, 1, 128), F32),
             pltpu.VMEM((2 * heads, F), BF16),
             dma((7,)),
             dma((steps,)),
+            dma((2, 2)),
             dma((2,)),
-            dma((2,)),
-            dma((4, steps)),
-            dma((4, steps)),
-            dma((steps,)),
-            dma((steps,)),
-            dma((steps,)),
+            dma((4, S)),
+            dma((4, S)),
+            dma((S,)),
+            dma((S,)),
             dma((n * m,)),
             dma((n * m,)),
         ],
@@ -770,7 +821,17 @@
             collective_id=0, has_side_effects=True, vmem_limit_bytes=56 * 1024 * 1024
         ),
     )(*flat)
-    return cache.reshape(S, heads, R, STATE), read.reshape(S, heads, R)
+    cache, read = pl.pallas_call(
+        lambda *refs: emit_kernel((heads, R), *refs),
+        out_shape=(
+            jax.ShapeDtypeStruct((S, RH, STATE), BF16),
+            jax.ShapeDtypeStruct((S, heads, R), BF16),
+        ),
+        in_specs=[vmem, vmem],
+        out_specs=(pl.BlockSpec(memory_space=pltpu.HBM), vmem),
+        scratch_shapes=[dma],
+    )(on_chip(cache), on_chip(read))
+    return cache.reshape(S, heads, R, STATE), read
 
 
 def fits(n, m, shapes):

time: 80.8 us -> 46 us (0.57)
  Pallas kernels: 76.8 us -> 45.1 us
  local copies, waits for them, and re-layouts: 3.14 us -> 0 us
    pallas_call x1 -> x2, Pallas kernels: 76.8 us -> 45.1 us  [the longest x1 43.7 us: fused(): pl.pallas_call(lambda *refs: mixer_kernel(dims, *refs), out_shape=(pltpu....]
    unnamed x1 -> x0, local copies, waits for them, and re-layouts: 1.77 us -> none
    reshape x1 -> x0, local copies, waits for them, and re-layouts: 1.37 us -> none  [fused(): return (cache.reshape(S, heads, R, STATE), read.reshape(S, heads, R))]
where the time goes in v2:
time: 46 us; the launch traced here: 45.7 us
  Pallas kernels  45.1 us (98%)
  between operations  0.64 us (1%)
    pallas_call x1, Pallas kernels, fused(): pl.pallas_call(lambda *refs: mixer_kernel(dims, *refs), out_shape=(pltpu....  43.7 us
    pallas_call x1, Pallas kernels, fused(): pl.pallas_call(lambda *refs: emit_kernel((heads, R), *refs), out_shape=(j...  1.36 us

profile of v2, /device:TPU:0, one launch (start us, length us, event | category | flops | bytes accessed | tf_op | source)
XLA Modules:
  0.0 45.7 jit_solution(9143428659177137682)
XLA Ops:
  0.6 43.7 %shard_map.158 = (bf16[12,128,128]{2,1,0:T(8,128)(2,1)S(1)}, bf16[12,128]{1,0:T(8,128)(2,1)S(1)}) custom-call(bf16[12,128,2048]{2,1,0:T(8,128)(2,1)} %refs_0_.1, bf16[12,2048]{1,0:T(8,128)(2,1)} %refs_1_.1, bf16[2048,512]{1,0:T(8,128)(2,1)} %refs_2_.1, bf16[2048,512]{1,0:T(8,128)(2,1)} %refs_3_.1, bf16[2048,256]{1,0:T(8,128)(2,1)} %refs_4_.1, ...), custom_call_target="tpu_custom_call" | custom-call | tf_op jit(solution)/shard_map/pallas_call | solution.py:777
  44.4 1.4 %shard_map.159 = (bf16[12,128,128]{2,1,0:T(8,128)(2,1)}, bf16[12,8,16]{2,1,0:T(8,128)(2,1)}) custom-call(bf16[12,128,128]{2,1,0:T(8,128)(2,1)S(1)} %get-tuple-element.6.refs_0_, bf16[12,128]{1,0:T(8,128)(2,1)S(1)} %get-tuple-element.7.refs_1_), custom_call_target="tpu_custom_call" | custom-call | tf_op jit(solution)/shard_map/pallas_call | solution.py:824

commit v3 on v2

--- a/solution.py
+++ b/solution.py
@@ -200,12 +200,23 @@
 def mixer_kernel(
     dims,
     x_hbm,
-    next_ref,
+    next_hbm,
     wv_hbm,
     wg_hbm,
     wk_hbm,
     wq_hbm,
     ws_hbm,
+    tv_hbm,
+    tk_hbm,
+    tq_hbm,
+    bias_hbm,
+    speed_hbm,
+    skip_hbm,
+    gain_hbm,
+    off_hbm,
+    cache_ref,
+    read_ref,
+    next_ref,
     tv_ref,
     tk_ref,
     tq_ref,
@@ -213,9 +224,6 @@
     speed_ref,
     skip_ref,
     gain_ref,
-    off_hbm,
-    cache_ref,
-    read_ref,
     xbuf,
     edge,
     wall,
@@ -245,10 +253,10 @@
     new_sem,
     st_send,
     st_recv,
+    near_recv,
     log_send,
     log_recv,
-    sq_send,
-    sq_recv,
+    sq_sem,
 ):
     n, m, S, L, heads, R, G = dims
     F = heads * P_SIZE
@@ -268,35 +276,72 @@
         c.start()
         return c
 
-    def load_x(g):
-        return pltpu.make_async_copy(
-            x_hbm.at[pl.ds(g * G, G)], xbuf.at[pl.ds(g * G, G)], x_sem.at[g]
-        )
-
-    peers = [(a, b) for a in range(n) for b in range(m) if (a, b) != (0, 0)]
-
-    def at(a, b=0):
-        return {"sp": lax.rem(me + a, n), "tp": lax.rem(tp + b, m)}
-
-    barrier = pltpu.get_barrier_semaphore()
-    for a, b in peers:
-        pl.semaphore_signal(barrier, inc=1, device_id=at(a, b), device_id_type=MESH)
+    def load_x(k):
+        here = pl.ds(0, G) if k == 0 else pl.ds(G, S - G)
+        return pltpu.make_async_copy(x_hbm.at[here], xbuf.at[here], x_sem.at[k])
 
     first = [
         load(ws_hbm.at[pl.ds(lead, heads), :], ws, 0),
         load(x_hbm.at[:, pl.ds(L - 16, 16)], edge.at[pl.ds(0, S)], 1),
         load(wk_hbm.at[:, pl.ds(gcol, STATE)], wall.at[:, pl.ds(128 + F, STATE)], 2),
         load(wq_hbm.at[:, pl.ds(gcol, STATE)], wall.at[:, pl.ds(128 + C, STATE)], 3),
-        load(wv_hbm, wall.at[:, pl.ds(128, F)], 4),
     ]
-
+    strips = 2 if F % 512 == 0 else 1
+    width = F // strips
+    first += [
+        load(
+            wv_hbm.at[:, pl.ds(k * width, width)],
+            wall.at[:, pl.ds(128 + k * width, width)],
+            4 + k,
+        )
+        for k in range(strips)
+    ]
+    small = [
+        load(a, b, 8 + k)
+        for k, (a, b) in enumerate(
+            [
+                (next_hbm, next_ref),
+                (tv_hbm, tv_ref),
+                (tk_hbm, tk_ref),
+                (tq_hbm, tq_ref),
+                (bias_hbm, bias_ref),
+                (speed_hbm, speed_ref),
+                (skip_hbm, skip_ref),
+                (gain_hbm, gain_ref),
+            ]
+        )
+    ]
+
+    peers = [(a, b) for a in range(n) for b in range(m) if (a, b) != (0, 0)]
+
+    def at(a, b=0):
+        return {"sp": lax.rem(me + a, n), "tp": lax.rem(tp + b, m)}
+
+    barrier = pltpu.get_barrier_semaphore()
+    for a, b in peers:
+        pl.semaphore_signal(barrier, inc=1, device_id=at(a, b), device_id_type=MESH)
+
+    head_of = ones_where((heads, F), lambda i, c: i == lax.div(c, P_SIZE))
+    expand[...] = jnp.concatenate([head_of, head_of], axis=0).astype(BF16)
+    @pl.when(me == 0)
+    def _():
+        from_left[:, 0] = jnp.zeros((S, RH, STATE), BF16)
+
+    @pl.when(me == n - 1)
+    def _():
+        from_right[:, n - 1] = jnp.zeros((S, RH, STATE), BF16)
+        log_in[...] = jnp.zeros_like(log_in)
+
+    eye = ones_where((heads, 128), lambda i, c: i == c)
+    later_ones = ones_where((L, L), lambda u, t: u > t, BF16)
+
+    for c in small:
+        c.wait()
     taps[:, 0:F] = tv_ref[:, pl.ds(fcol, F)].astype(F32)
     taps[:, F:C] = tk_ref[:, pl.ds(gcol, STATE)].astype(F32)
     taps[:, C : C + STATE] = tq_ref[:, pl.ds(gcol, STATE)].astype(F32)
     edge[S] = jnp.zeros(edge.shape[1:], BF16)
     edge[S, 0:S, :] = next_ref[...]
-    head_of = ones_where((heads, F), lambda i, c: i == lax.div(c, P_SIZE))
-    expand[...] = jnp.concatenate([head_of, head_of], axis=0).astype(BF16)
     bias = bias_ref[...]
     speed = jnp.exp(speed_ref[...])
     square = jnp.zeros((128, 128 - HEADS), F32)
@@ -308,37 +353,33 @@
 
     bias_t, speed_t = columns(bias, 0), columns(speed, 1)
 
-    @pl.when(me == 0)
-    def _():
-        from_left[:, 0] = jnp.zeros((S, RH, STATE), BF16)
-
-    @pl.when(me == n - 1)
-    def _():
-        from_right[:, n - 1] = jnp.zeros((S, RH, STATE), BF16)
-        log_in[...] = jnp.zeros_like(log_in)
-
-    eye = ones_where((heads, 128), lambda i, c: i == c)
-    later_ones = ones_where((L, L), lambda u, t: u > t, BF16)
-
     for c in first[1:4]:
         c.wait()
     load_x(0).start()
-    first[4].wait()
-    off_load = load(off_hbm.at[:, pl.ds(lead, heads), :], off, 5)
+    off_load = load(off_hbm.at[:, pl.ds(lead, heads), :], off, 6)
     rows = edge[...].reshape((S + 1) * 16, edge.shape[2])
-    eproj = jnp.dot(rows, wall[:, 128:], preferred_element_type=F32).astype(BF16).astype(F32)
-    e3 = eproj.reshape(S + 1, 16, C + STATE)
-    new_raw = e3[S]
-    tail_rows = halo_out.shape[1] - G * (CONV - 1)
-    for g in range(steps):
-        tails = [e3[g * G + q, 16 - (CONV - 1) :, 0:C] for q in range(G)]
-        if tail_rows:
-            tails.append(jnp.zeros((tail_rows, C), F32))
-        halo_out[g] = jnp.concatenate(tails, axis=0).astype(BF16)
-
-    for g in range(1, steps):
-        load_x(g).start()
-    gate_load = load(wg_hbm, wg, 6)
+    halo_out[...] = jnp.zeros_like(halo_out)
+    parts = {}
+
+    def edges(a, b):
+        part = jnp.dot(rows, wall[:, 128 + a : 128 + b], preferred_element_type=F32)
+        parts[a] = part.astype(BF16).astype(F32).reshape(S + 1, 16, b - a)
+        tails(a, range(G))
+
+    def tails(a, prompts):
+        c = min(a + parts[a].shape[2], C)
+        for p in prompts:
+            r = p % G * (CONV - 1)
+            tail = parts[a][p, 16 - (CONV - 1) :, 0 : c - a]
+            halo_out[p // G, r : r + CONV - 1, a:c] = tail.astype(BF16)
+
+    edges(F, C + STATE)
+    for k in range(strips):
+        first[4 + k].wait()
+        edges(k * width, (k + 1) * width)
+    if steps > 1:
+        load_x(1).start()
+    gate_load = load(wg_hbm, wg, 7)
     pl.semaphore_wait(barrier, len(peers))
 
     def halo_copy(k):
@@ -356,13 +397,15 @@
 
     @pl.when(me < n - 1)
     def _():
-        for k in halo_parts:
+        halo_copy(0).start()
+
+    for a in parts:
+        tails(a, range(G, S))
+
+    @pl.when(me < n - 1)
+    def _():
+        for k in halo_parts[1:]:
             halo_copy(k).start()
-
-    first[0].wait()
-    wall[:, 0:128] = jnp.concatenate(
-        [ws[...], jnp.zeros((128 - heads, ws.shape[1]), BF16)], axis=0
-    ).T
 
     def newest_copy():
         return pltpu.make_async_remote_copy(
@@ -374,43 +417,114 @@
             device_id_type=MESH,
         )
 
+    order = sorted(parts)
+    last = 16 - (CONV - 1)
+
+    @pl.when(me == n - 1)
+    def _():
+        newest[...] = jnp.zeros_like(newest)
+        for a in order:
+            b = a + parts[a].shape[2]
+            newest[0:S, a:b] = sum(
+                parts[a][0:S, last + j, :] * taps[j : j + 1, a:b] for j in range(CONV - 1)
+            )
+        newest_copy().start()
+
+    new_raw = jnp.concatenate([parts[a][S] for a in order], axis=1)
+    first[0].wait()
+    wall[:, 0:128] = jnp.concatenate(
+        [ws[...], jnp.zeros((128 - heads, ws.shape[1]), BF16)], axis=0
+    ).T
+
     def span(s, right, far):
         if right:
             return (s + 2, n) if far else (s + 1, s + 2)
         return (0, s - 1) if far else (s - 1, s)
 
-    def flow(p, s, right, far):
-        lo, hi = span(s, right, far)
-        if not (0 <= lo < hi <= n):
-            return None
-        k = 2 * int(right) + int(far)
-        here = (p, pl.ds(lo, hi - lo))
+    def is_end(s, right):
+        return s == (0 if right else n - 1)
+
+    def kinds(s, right):
+        if not 0 <= (s + 1 if right else s - 1) < n:
+            return ()
+        if is_end(s, right):
+            return (FAR, NEAR) if n > 2 else (NEAR,)
+        return (FINAL,) if (s + 1 == n - 1 if right else s - 1 == 0) else (FAR, NEAR)
+
+    def message(i, s, right, kind):
+        lo, hi = span(s, right, kind == FAR)
+        here = (pl.ds(i * G, G) if kind == NEAR else i, pl.ds(lo, hi - lo))
+        lane = 0 if is_end(s, right) else 1
         return pltpu.make_async_remote_copy(
             own.at[here],
             (from_left if right else from_right).at[here],
-            st_send.at[k, p],
-            st_recv.at[k, p],
+            st_send.at[kind, lax.rem(i, RING)],
+            (near_recv if kind == NEAR else st_recv).at[lane, i],
             device_id=at(1 if right else n - 1),
             device_id_type=MESH,
         )
 
-    def begin(p, s, right, far):
-        c = flow(p, s, right, far)
-        if c is not None:
-            c.start()
-
-    def log_copy(p):
+    def flight(s, right, kind):
+        return END_NEARS if kind == NEAR and is_end(s, right) else RING
+
+    def send(i, s, right, kind):
+        depth = flight(s, right, kind)
+
+        @pl.when(i >= depth)
+        def _():
+            message(i - depth, s, right, kind).wait_send()
+
+        message(i, s, right, kind).start()
+
+    def drain(s, right):
+        for kind in kinds(s, right):
+            total = steps if kind == NEAR else S
+            for i in range(max(0, total - flight(s, right, kind)), total):
+                message(i, s, right, kind).wait_send()
+
+    def send_prompt(g, q, s, right):
+        behind = END_BEHIND if is_end(s, right) else MID_BEHIND
+        for kind in kinds(s, right):
+            if kind != NEAR:
+                send(g * G + q, s, right, kind)
+            elif q == G - 1:
+
+                @pl.when(g >= behind)
+                def _():
+                    send(g - behind, s, right, NEAR)
+
+    def send_rest(s, right):
+        behind = END_BEHIND if is_end(s, right) else MID_BEHIND
+        if NEAR in kinds(s, right):
+
+            def one(g, carry):
+                send(g, s, right, NEAR)
+                return carry
+
+            lax.fori_loop(max(0, steps - behind), steps, one, 0)
+
+    def log_copy(g):
+        here = pl.ds(g * G, G)
         return pltpu.make_async_remote_copy(
-            log_out.at[p],
-            log_in.at[p],
-            log_send.at[p],
-            log_recv.at[p],
+            log_out.at[here],
+            log_in.at[here],
+            log_send.at[g],
+            log_recv.at[g],
             device_id=at(n - 1),
             device_id_type=MESH,
         )
 
     def project(g):
-        load_x(g).wait()
+        @pl.when(g == 0)
+        def _():
+            load_x(0).wait()
+
+        if steps > 1:
+
+            @pl.when(g == 1)
+            def _():
+                load_x(1).wait()
+
         slot = lax.rem(g, lead_steps)
         xg = xbuf[pl.ds(g * G, G)].reshape(G * L, xbuf.shape[2])
         acc = jnp.dot(xg, wall[:, 0 : 128 + C], preferred_element_type=F32).astype(BF16).astype(F32)
@@ -432,37 +546,16 @@
             hi = w.astype(BF16).astype(F32)
             wsplit[slot, q] = jnp.concatenate([hi, w - hi], axis=0).astype(BF16)
 
-    depth, behind = min(DEPTH, S), min(BEHIND, S)
-
-    def feed(p, s, right):
-        if flow(0, s, right, True) is not None:
-
-            @pl.when((p >= depth) & (p < S + depth))
-            def _():
-                flow(p - depth, s, right, True).wait_send()
-
-            @pl.when(p < S)
-            def _():
-                begin(p, s, right, True)
-
-        @pl.when(p >= depth + behind)
-        def _():
-            flow(p - depth - behind, s, right, False).wait_send()
-
-        @pl.when(p >= behind)
-        def _():
-            begin(p - behind, s, right, False)
-
-    def feed_rest(s, right):
-        def one(p, carry):
-            feed(p, s, right)
-            return carry
-
-        lax.fori_loop(S, S + behind, one, 0)
-
     def states(g):
         slot = lax.rem(g, lead_steps)
         before = halo_in[g].astype(F32)
+
+        @pl.when(me == n - 1)
+        def _():
+            for q in range(G):
+                log_out[g * G + q] = log_own[g * G + q]
+            log_copy(g).start()
+
         for q in range(G):
             p = g * G + q
             pad[slot, q, 8 - (CONV - 1) : 8, :] = before[q * (CONV - 1) : (q + 1) * (CONV - 1)]
@@ -494,43 +587,44 @@
                         own[p, d, h * R : (h + 1) * R, :] = share[b : b + R]
 
             @pl.when(me == 0)
-            def _(p=p):
-                feed(p, 0, True)
+            def _(q=q):
+                send_prompt(g, q, 0, True)
 
             @pl.when(me == n - 1)
-            def _(p=p):
-                log_out[p] = log_own[p]
-                log_copy(p).start()
-                feed(p, n - 1, False)
+            def _(q=q):
+                send_prompt(g, q, n - 1, False)
 
     def later_factor(p):
         row = jnp.sum(eye * log_in[p], axis=1, keepdims=True)
         return jnp.exp(jnp.broadcast_to(row, (heads, 128)))
 
-    def sum_right(p, s):
-        flow(p, s - 1, True, True).wait_recv()
+    def sum_right(g, q, s):
+        p = g * G + q
+        message(p, s - 1, True, FAR).wait_recv()
         factor = decay[p]
         for d in reversed(range(s + 1, n)):
             for h in range(heads):
                 z = (p, d, slice(h * R, (h + 1) * R))
                 got = from_left[z].astype(F32) * factor[h : h + 1, :]
                 own[z] = (own[z].astype(F32) + got).astype(BF16)
-        begin(p, s, True, True)
-        begin(p, s, True, False)
-
-    def sum_left(p, s):
-        log_copy(p).wait_recv()
-        log_out[p] = log_in[p] + log_own[p]
-        log_copy(p).start()
-        flow(p, s + 1, False, True).wait_recv()
+        send_prompt(g, q, s, True)
+
+    def sum_left(g, q, s):
+        p = g * G + q
+        message(p, s + 1, False, FAR).wait_recv()
         factor = later_factor(p)
         for d in range(s):
             for h in range(heads):
                 z = (p, d, slice(h * R, (h + 1) * R))
                 mine = own[z].astype(F32) * factor[h : h + 1, :]
                 own[z] = (from_right[z].astype(F32) + mine).astype(BF16)
-        begin(p, s, False, True)
-        begin(p, s, False, False)
+        send_prompt(g, q, s, False)
+
+    def pass_log(g):
+        log_copy(g).wait_recv()
+        for q in range(G):
+            log_out[g * G + q] = log_in[g * G + q] + log_own[g * G + q]
+        log_copy(g).start()
 
     def relay(g, outer):
         for s in range(1, n - 1):
@@ -539,22 +633,12 @@
             def _(s=s):
                 for q in range(G):
                     if outer == (s < n - 1 - s):
-                        sum_right(g * G + q, s)
+                        sum_right(g, q, s)
                     else:
-                        sum_left(g * G + q, s)
+                        sum_left(g, q, s)
 
     off_load.wait()
     lax.fori_loop(0, lead_steps, lambda g, carry: (project(g), carry)[1], 0)
-    @pl.when(me == n - 1)
-    def _():
-        total = jnp.zeros((S, C + STATE), F32)
-        for j in range(CONV - 1):
-            row = 16 - (CONV - 1) + j
-            total = total + e3[0:S, row, :] * taps[j : j + 1, :]
-        newest[...] = jnp.zeros_like(newest)
-        newest[0:S, :] = total
-        newest_copy().start()
-
     @pl.when(me == 0)
     def _():
         halo_in[...] = jnp.zeros_like(halo_in)
@@ -586,6 +670,12 @@
                 def _():
                     newest_copy().wait_recv()
                     newest_copy().start()
+
+        for s in range(1, n - 1):
+
+            @pl.when((me == s) & (g >= n - 2 - s))
+            def _(s=s):
+                pass_log(g - (n - 2 - s))
 
         @pl.when(g >= relay_lag)
         def _():
@@ -626,27 +716,33 @@
     both = jnp.sum(new_in * new_out.astype(F32), axis=1, keepdims=True)
     where_row = lax.broadcasted_iota(jnp.int32, (SP, RH), 0)
 
-    @pl.when(me == 0)
-    def _():
-        feed_rest(0, True)
-
-    @pl.when(me == n - 1)
-    def _():
-        feed_rest(n - 1, False)
+    def rest(outer):
+        for s in range(n):
+            for right in (True, False):
+                if outer == (is_end(s, right) or (s < n - 1 - s) == right):
+
+                    @pl.when(me == s)
+                    def _(s=s, right=right):
+                        send_rest(s, right)
+
+    def arrivals(g, s, right):
+        if FINAL in kinds(s, right):
+            for q in range(G):
+                message(g * G + q, s, right, FINAL).wait_recv()
+        elif NEAR in kinds(s, right):
+            message(g, s, right, NEAR).wait_recv()
 
     def finish(g, y):
         for s in range(n):
 
             @pl.when(me == s)
             def _(s=s):
-                for q in range(G):
-                    p = g * G + q
-                    if s > 0:
-                        flow(p, s - 1, True, False).wait_recv()
-                    if s == 0:
-                        log_copy(p).wait_recv()
-                    if s < n - 1:
-                        flow(p, s + 1, False, False).wait_recv()
+                if s > 0:
+                    arrivals(g, s - 1, True)
+                if s == 0:
+                    log_copy(g).wait_recv()
+                if s < n - 1:
+                    arrivals(g, s + 1, False)
 
         for q in range(G):
             p = g * G + q
@@ -665,11 +761,20 @@
             y = jnp.where(where_row == p, part, y)
         return y
 
+    for s in range(1, n - 2):
+
+        @pl.when(me == s)
+        def _(s=s):
+            for g in range(max(0, steps - (n - 2 - s)), steps):
+                pass_log(g)
+
     for g in range(steps - relay_lag, steps):
         relay(g, True)
         if g > 0:
             relay(g - 1, False)
+    rest(True)
     relay(steps - 1, False)
+    rest(False)
     y = lax.fori_loop(0, steps, finish, jnp.zeros((SP, RH), F32))
 
     readout = keep_here * y + dt_here * new_input * both + skip_here * new_input
@@ -682,34 +787,23 @@
     def sq_copy(i):
         a, b = peers[i]
         return pltpu.make_async_remote_copy(
-            sq_out, sq_in.at[i], sq_send.at[i], sq_recv.at[i], device_id=at(a, b), device_id_type=MESH
+            sq_out, sq_in.at[i], sq_sem.at[0], sq_sem.at[1], device_id=at(a, b), device_id_type=MESH
         )
 
+    all_squares = pltpu.make_async_remote_copy(
+        sq_in, sq_in, sq_sem.at[0], sq_sem.at[1], device_id=at(1), device_id_type=MESH
+    )
     for i in range(len(peers)):
         sq_copy(i).start()
     for s in range(n):
 
         @pl.when(me == s)
         def _(s=s):
-            end = s in (0, n - 1)
-
-            def sent(p, carry):
-                for right in (False, True):
-                    for far in (False, True):
-                        c = flow(p, s, right, far)
-                        if c is None:
-                            continue
-                        fed = p < S + min(0, behind - depth) if far else p < S - depth
-
-                        @pl.when(jnp.logical_not(fed & end))
-                        def _(c=c):
-                            c.wait_send()
-
-                if s > 0:
-                    log_copy(p).wait_send()
-                return carry
-
-            lax.fori_loop(0, S, sent, 0)
+            drain(s, True)
+            drain(s, False)
+            if s > 0:
+                for g in range(steps):
+                    log_copy(g).wait_send()
 
     @pl.when(me < n - 1)
     def _():
@@ -720,37 +814,44 @@
     def _():
         newest_copy().wait_send()
 
+    all_squares.wait_recv()
     for i in range(len(peers)):
-        sq_copy(i).wait_recv()
         sq = sq + sq_in[i]
     mean = jnp.sum(diagonal * sq, axis=1, keepdims=True) / (HEADS * P_SIZE)
     scale = lax.rsqrt(mean + epsilon)
     read_ref[...] = (gated * scale * gain_here).astype(BF16)[0:S]
 
-    for i in range(len(peers)):
-        sq_copy(i).wait_send()
+    all_squares.wait_send()
 
 
 def on_chip(array):
     return pltpu.with_memory_space_constraint(array, pltpu.VMEM)
 
 
-def emit_kernel(dims, cache_ref, read_ref, cache_hbm, out_ref, sem):
+def emit_kernel(dims, cache_ref, read_ref, cache_hbm, out_hbm, out, sem):
     heads, R = dims
     S, RH = read_ref.shape
-    copy = pltpu.make_async_copy(cache_ref, cache_hbm, sem)
-    copy.start()
+    copies = [
+        pltpu.make_async_copy(cache_ref, cache_hbm, sem.at[0]),
+        pltpu.make_async_copy(out, out_hbm, sem.at[1]),
+    ]
+    copies[0].start()
     spread = ones_where((heads, RH), lambda h, l: h == lax.div(l, R))
     pick = ones_where((RH, R), lambda l, r: lax.rem(l, R) == r, BF16)
     value = read_ref[...].astype(F32)
     rows = jnp.concatenate([value[p : p + 1] * spread for p in range(S)], axis=0).astype(BF16)
-    out = jnp.dot(rows, pick, preferred_element_type=F32)
-    out_ref[...] = out.reshape(S, heads, R).astype(BF16)
-    copy.wait()
+    picked = jnp.dot(rows, pick, preferred_element_type=F32)
+    out[...] = picked.reshape(S, heads, R).astype(BF16)
+    copies[1].start()
+    for c in copies:
+        c.wait()
 
 
 LEAD, RELAY_LAG, FORWARD_AT = 1, 1, 2
-DEPTH, BEHIND = 4, 8
+FAR, NEAR, FINAL = 0, 1, 2
+SMALL = (1, 7, 8, 9, 10, 11, 12, 13)
+RING, END_NEARS = 4, 2
+END_BEHIND, MID_BEHIND = 5, 2
 
 
 def fused(*args):
@@ -772,7 +873,7 @@
     flat[6] = args[6].T
     flat[14] = jnp.swapaxes(args[14], 1, 2)
     hbm, vmem = pl.BlockSpec(memory_space=pl.ANY), pl.BlockSpec(memory_space=pltpu.VMEM)
-    specs = [hbm, vmem, hbm, hbm, hbm, hbm, hbm] + [vmem] * 7 + [hbm]
+    specs = [hbm] * len(flat)
     dma = pltpu.SemaphoreType.DMA
     cache, read = pl.pallas_call(
         lambda *refs: mixer_kernel(dims, *refs),
@@ -783,6 +884,7 @@
         in_specs=specs,
         out_specs=(vmem, vmem),
         scratch_shapes=[
+            *[pltpu.VMEM(flat[i].shape, flat[i].dtype) for i in SMALL],
             pltpu.VMEM((S, L, D), BF16),
             pltpu.VMEM((S + 1, 16, D), BF16),
             pltpu.VMEM((D, 128 + C + STATE), BF16),
@@ -806,16 +908,16 @@
             pltpu.VMEM((1, 128), F32),
             pltpu.VMEM((n * m - 1, 1, 128), F32),
             pltpu.VMEM((2 * heads, F), BF16),
-            dma((7,)),
-            dma((steps,)),
+            dma((16,)),
+            dma((2,)),
             dma((2, 2)),
             dma((2,)),
-            dma((4, S)),
-            dma((4, S)),
-            dma((S,)),
-            dma((S,)),
-            dma((n * m,)),
-            dma((n * m,)),
+            dma((3, RING)),
+            dma((2, S)),
+            dma((2, steps)),
+            dma((steps,)),
+            dma((steps,)),
+            dma((2,)),
         ],
         compiler_params=pltpu.CompilerParams(
             collective_id=0, has_side_effects=True, vmem_limit_bytes=56 * 1024 * 1024
@@ -828,8 +930,8 @@
             jax.ShapeDtypeStruct((S, heads, R), BF16),
         ),
         in_specs=[vmem, vmem],
-        out_specs=(pl.BlockSpec(memory_space=pltpu.HBM), vmem),
-        scratch_shapes=[dma],
+        out_specs=(pl.BlockSpec(memory_space=pltpu.HBM),) * 2,
+        scratch_shapes=[pltpu.VMEM((S, heads, R), BF16), dma((2,))],
     )(on_chip(cache), on_chip(read))
     return cache.reshape(S, heads, R, STATE), read
 

time: 46 us -> 43.5 us (0.946)
  Pallas kernels: 45.1 us -> 42.6 us
    pallas_call x1, Pallas kernels: 43.7 us -> 41.8 us  [fused(): pl.pallas_call(lambda *refs: mixer_kernel(dims, *refs), out_shape=(pltpu....]
    pallas_call x1, Pallas kernels: 1.36 us -> 0.77 us  [fused(): pl.pallas_call(lambda *refs: emit_kernel((heads, R), *refs), out_shape=(j...]
where the time goes in v3:
time: 43.5 us; the launch traced here: 43.2 us
  Pallas kernels  42.6 us (98%)
  between operations  0.64 us (1%)
    pallas_call x1, Pallas kernels, fused(): pl.pallas_call(lambda *refs: mixer_kernel(dims, *refs), out_shape=(pltpu....  41.8 us

profile of v3, /device:TPU:0, one launch (start us, length us, event | category | flops | bytes accessed | tf_op | source)
XLA Modules:
  0.0 43.2 jit_solution(12216824396489363526)
XLA Ops:
  0.6 41.8 %shard_map.158 = (bf16[12,128,128]{2,1,0:T(8,128)(2,1)S(1)}, bf16[12,128]{1,0:T(8,128)(2,1)S(1)}) custom-call(bf16[12,128,2048]{2,1,0:T(8,128)(2,1)} %refs_0_.1, bf16[12,2048]{1,0:T(8,128)(2,1)} %refs_1_.1, bf16[2048,512]{1,0:T(8,128)(2,1)} %refs_2_.1, bf16[2048,512]{1,0:T(8,128)(2,1)} %refs_3_.1, bf16[2048,256]{1,0:T(8,128)(2,1)} %refs_4_.1, ...), custom_call_target="tpu_custom_call" | custom-call | tf_op jit(solution)/shard_map/pallas_call | solution.py:878
  42.4 0.8 %shard_map.159 = (bf16[12,128,128]{2,1,0:T(8,128)(2,1)}, bf16[12,8,16]{2,1,0:T(8,128)(2,1)}) custom-call(bf16[12,128,128]{2,1,0:T(8,128)(2,1)S(1)} %get-tuple-element.6.refs_0_, bf16[12,128]{1,0:T(8,128)(2,1)S(1)} %get-tuple-element.7.refs_1_), custom_call_target="tpu_custom_call" | custom-call | tf_op jit(solution)/shard_map/pallas_call | solution.py:926

commit v4 on v3

--- a/solution.py
+++ b/solution.py
@@ -285,16 +285,7 @@
         load(x_hbm.at[:, pl.ds(L - 16, 16)], edge.at[pl.ds(0, S)], 1),
         load(wk_hbm.at[:, pl.ds(gcol, STATE)], wall.at[:, pl.ds(128 + F, STATE)], 2),
         load(wq_hbm.at[:, pl.ds(gcol, STATE)], wall.at[:, pl.ds(128 + C, STATE)], 3),
-    ]
-    strips = 2 if F % 512 == 0 else 1
-    width = F // strips
-    first += [
-        load(
-            wv_hbm.at[:, pl.ds(k * width, width)],
-            wall.at[:, pl.ds(128 + k * width, width)],
-            4 + k,
-        )
-        for k in range(strips)
+        load(wv_hbm, wall.at[:, pl.ds(128, F)], 4),
     ]
     small = [
         load(a, b, 8 + k)
@@ -359,24 +350,17 @@
     off_load = load(off_hbm.at[:, pl.ds(lead, heads), :], off, 6)
     rows = edge[...].reshape((S + 1) * 16, edge.shape[2])
     halo_out[...] = jnp.zeros_like(halo_out)
-    parts = {}
-
-    def edges(a, b):
-        part = jnp.dot(rows, wall[:, 128 + a : 128 + b], preferred_element_type=F32)
-        parts[a] = part.astype(BF16).astype(F32).reshape(S + 1, 16, b - a)
-        tails(a, range(G))
-
-    def tails(a, prompts):
-        c = min(a + parts[a].shape[2], C)
+    first[4].wait()
+    part = jnp.dot(rows, wall[:, 128:], preferred_element_type=F32)
+    edge_rows = part.astype(BF16).astype(F32).reshape(S + 1, 16, C + STATE)
+
+    def tails(prompts):
         for p in prompts:
             r = p % G * (CONV - 1)
-            tail = parts[a][p, 16 - (CONV - 1) :, 0 : c - a]
-            halo_out[p // G, r : r + CONV - 1, a:c] = tail.astype(BF16)
-
-    edges(F, C + STATE)
-    for k in range(strips):
-        first[4 + k].wait()
-        edges(k * width, (k + 1) * width)
+            tail = edge_rows[p, 16 - (CONV - 1) :, 0:C]
+            halo_out[p // G, r : r + CONV - 1, :] = tail.astype(BF16)
+
+    tails(range(G))
     if steps > 1:
         load_x(1).start()
     gate_load = load(wg_hbm, wg, 7)
@@ -399,8 +383,7 @@
     def _():
         halo_copy(0).start()
 
-    for a in parts:
-        tails(a, range(G, S))
+    tails(range(G, S))
 
     @pl.when(me < n - 1)
     def _():
@@ -417,20 +400,17 @@
             device_id_type=MESH,
         )
 
-    order = sorted(parts)
     last = 16 - (CONV - 1)
 
     @pl.when(me == n - 1)
     def _():
         newest[...] = jnp.zeros_like(newest)
-        for a in order:
-            b = a + parts[a].shape[2]
-            newest[0:S, a:b] = sum(
-                parts[a][0:S, last + j, :] * taps[j : j + 1, a:b] for j in range(CONV - 1)
-            )
+        newest[0:S, :] = sum(
+            edge_rows[0:S, last + j, :] * taps[j : j + 1, :] for j in range(CONV - 1)
+        )
         newest_copy().start()
 
-    new_raw = jnp.concatenate([parts[a][S] for a in order], axis=1)
+    new_raw = edge_rows[S]
     first[0].wait()
     wall[:, 0:128] = jnp.concatenate(
         [ws[...], jnp.zeros((128 - heads, ws.shape[1]), BF16)], axis=0
@@ -548,7 +528,6 @@
 
     def states(g):
         slot = lax.rem(g, lead_steps)
-        before = halo_in[g].astype(F32)
 
         @pl.when(me == n - 1)
         def _():
@@ -558,7 +537,6 @@
 
         for q in range(G):
             p = g * G + q
-            pad[slot, q, 8 - (CONV - 1) : 8, :] = before[q * (CONV - 1) : (q + 1) * (CONV - 1)]
             wide = lax.dot_general(
                 wsplit[slot, q],
                 expand[...],
@@ -566,17 +544,32 @@
                 preferred_element_type=F32,
             )
 
-            def mixed(c):
+            def mixed(c, a, b):
                 s = slice(c, c + 128)
-                t = pad[slot, q, 8 - (CONV - 1) : 8 - (CONV - 1) + L, s] * taps[0:1, s]
-                for j in range(1, CONV):
+                t = jnp.zeros((b - a, 128), F32)
+                for j in range(CONV):
                     r = 8 - (CONV - 1) + j
-                    t = t + pad[slot, q, r : r + L, s] * taps[j : j + 1, s]
-                return silu(t).astype(BF16)
-
-            in_map = mixed(F)
+                    t = t + pad[slot, q, r + a : r + b, s] * taps[j : j + 1, s]
+                return silu(t).astype(BF16).astype(F32)
+
+            columns = range(0, C, 128)
+            later = [mixed(c, 8, L) for c in columns]
+            if q == 0:
+                for k in halo_parts:
+
+                    @pl.when((g == k) & (me > 0))
+                    def _(k=k):
+                        halo_copy(k).wait_recv()
+
+            r = q * (CONV - 1)
+            pad[slot, q, 8 - (CONV - 1) : 8, :] = halo_in[g, r : r + CONV - 1, :].astype(F32)
+            whole = [
+                jnp.concatenate([mixed(c, 0, 8), late], axis=0)
+                for c, late in zip(columns, later)
+            ]
+            in_map = whole[-1].astype(BF16)
             for c in range(0, F, 128):
-                weighted = (mixed(c).astype(F32) * wide[:, c : c + 128]).astype(BF16)
+                weighted = (whole[c // 128] * wide[:, c : c + 128]).astype(BF16)
                 share = lax.dot_general(
                     weighted, in_map, (((0,), (0,)), ((), ())), preferred_element_type=F32
                 ).astype(BF16)
@@ -643,19 +636,9 @@
     def _():
         halo_in[...] = jnp.zeros_like(halo_in)
 
-    @pl.when(me > 0)
-    def _():
-        halo_copy(0).wait_recv()
-
     relay_lag = min(RELAY_LAG, steps)
 
     def step(g, carry):
-        if steps > 1:
-
-            @pl.when((g == 1) & (me > 0))
-            def _():
-                halo_copy(1).wait_recv()
-
         states(g)
 
         @pl.when(g + lead_steps < steps)

time: 43.5 us -> 42.6 us (0.979)
  Pallas kernels: 42.6 us -> 41.7 us
    pallas_call x1, Pallas kernels: 41.8 us -> 41 us  [fused(): pl.pallas_call(lambda *refs: mixer_kernel(dims, *refs), out_shape=(pltpu....]
where the time goes in v4:
time: 42.6 us; the launch traced here: 42.4 us
  Pallas kernels  41.7 us (98%)
  between operations  0.64 us (2%)
    pallas_call x1, Pallas kernels, fused(): pl.pallas_call(lambda *refs: mixer_kernel(dims, *refs), out_shape=(pltpu....  41 us

profile of v4, /device:TPU:0, one launch (start us, length us, event | category | flops | bytes accessed | tf_op | source)
XLA Modules:
  0.0 42.4 jit_solution(14970644103876840034)
XLA Ops:
  0.6 41.0 %shard_map.158 = (bf16[12,128,128]{2,1,0:T(8,128)(2,1)S(1)}, bf16[12,128]{1,0:T(8,128)(2,1)S(1)}) custom-call(bf16[12,128,2048]{2,1,0:T(8,128)(2,1)} %refs_0_.1, bf16[12,2048]{1,0:T(8,128)(2,1)} %refs_1_.1, bf16[2048,512]{1,0:T(8,128)(2,1)} %refs_2_.1, bf16[2048,512]{1,0:T(8,128)(2,1)} %refs_3_.1, bf16[2048,256]{1,0:T(8,128)(2,1)} %refs_4_.1, ...), custom_call_target="tpu_custom_call" | custom-call | tf_op jit(solution)/shard_map/pallas_call | solution.py:861
  41.6 0.8 %shard_map.159 = (bf16[12,128,128]{2,1,0:T(8,128)(2,1)}, bf16[12,8,16]{2,1,0:T(8,128)(2,1)}) custom-call(bf16[12,128,128]{2,1,0:T(8,128)(2,1)S(1)} %get-tuple-element.6.refs_0_, bf16[12,128]{1,0:T(8,128)(2,1)S(1)} %get-tuple-element.7.refs_1_), custom_call_target="tpu_custom_call" | custom-call | tf_op jit(solution)/shard_map/pallas_call | solution.py:909

commit v5 on v4

--- a/solution.py
+++ b/solution.py
@@ -226,6 +226,7 @@
     gain_ref,
     xbuf,
     edge,
+    early,
     wall,
     ws,
     wg,
@@ -248,7 +249,6 @@
     sq_in,
     expand,
     load_sem,
-    x_sem,
     halo_sem,
     new_sem,
     st_send,
@@ -278,20 +278,30 @@
 
     def load_x(k):
         here = pl.ds(0, G) if k == 0 else pl.ds(G, S - G)
-        return pltpu.make_async_copy(x_hbm.at[here], xbuf.at[here], x_sem.at[k])
+        return pltpu.make_async_copy(x_hbm.at[here], xbuf.at[here], load_sem.at[k])
+
+    half = x_hbm.shape[2] // 2
+
+    def weights(k):
+        rows = pl.ds(k * half, half)
+        maps = pl.ds(gcol, STATE)
+        return [
+            load(wk_hbm.at[rows, maps], wall.at[rows, pl.ds(128 + F, STATE)], 10 + 3 * k),
+            load(wq_hbm.at[rows, maps], wall.at[rows, pl.ds(128 + C, STATE)], 11 + 3 * k),
+            load(wv_hbm.at[rows], wall.at[rows, pl.ds(128, F)], 12 + 3 * k),
+        ]
 
     first = [
-        load(ws_hbm.at[pl.ds(lead, heads), :], ws, 0),
-        load(x_hbm.at[:, pl.ds(L - 16, 16)], edge.at[pl.ds(0, S)], 1),
-        load(wk_hbm.at[:, pl.ds(gcol, STATE)], wall.at[:, pl.ds(128 + F, STATE)], 2),
-        load(wq_hbm.at[:, pl.ds(gcol, STATE)], wall.at[:, pl.ds(128 + C, STATE)], 3),
-        load(wv_hbm, wall.at[:, pl.ds(128, F)], 4),
+        load(next_hbm, next_ref, 0),
+        load(ws_hbm.at[pl.ds(lead, heads), :], ws, 8),
+        load(x_hbm.at[:, pl.ds(L - 16, 16)], edge.at[pl.ds(0, S)], 9),
     ]
+    first += weights(0)
+    second = weights(1)
     small = [
-        load(a, b, 8 + k)
+        load(a, b, 1 + k)
         for k, (a, b) in enumerate(
             [
-                (next_hbm, next_ref),
                 (tv_hbm, tv_ref),
                 (tk_hbm, tk_ref),
                 (tq_hbm, tq_ref),
@@ -326,32 +336,19 @@
     eye = ones_where((heads, 128), lambda i, c: i == c)
     later_ones = ones_where((L, L), lambda u, t: u > t, BF16)
 
-    for c in small:
+    for c in first:
         c.wait()
-    taps[:, 0:F] = tv_ref[:, pl.ds(fcol, F)].astype(F32)
-    taps[:, F:C] = tk_ref[:, pl.ds(gcol, STATE)].astype(F32)
-    taps[:, C : C + STATE] = tq_ref[:, pl.ds(gcol, STATE)].astype(F32)
     edge[S] = jnp.zeros(edge.shape[1:], BF16)
     edge[S, 0:S, :] = next_ref[...]
-    bias = bias_ref[...]
-    speed = jnp.exp(speed_ref[...])
-    square = jnp.zeros((128, 128 - HEADS), F32)
-
-    def columns(row, k):
-        full = jnp.concatenate([jnp.broadcast_to(row, (128, HEADS)), square], axis=1)
-        heads_t[k] = full.T[0:HEADS]
-        return heads_t[k, pl.ds(lead, heads), :]
-
-    bias_t, speed_t = columns(bias, 0), columns(speed, 1)
-
-    for c in first[1:4]:
+    rows = edge[...].reshape((S + 1) * 16, edge.shape[2])
+    halo_out[...] = jnp.zeros_like(halo_out)
+    early[...] = jnp.dot(rows[:, 0:half], wall[0:half, 128:], preferred_element_type=F32)
+    for c in second + small:
         c.wait()
     load_x(0).start()
-    off_load = load(off_hbm.at[:, pl.ds(lead, heads), :], off, 6)
-    rows = edge[...].reshape((S + 1) * 16, edge.shape[2])
-    halo_out[...] = jnp.zeros_like(halo_out)
-    first[4].wait()
-    part = jnp.dot(rows, wall[:, 128:], preferred_element_type=F32)
+    off_load = load(off_hbm.at[:, pl.ds(lead, heads), :], off, 2)
+    late = jnp.dot(rows[:, half:], wall[half:, 128:], preferred_element_type=F32)
+    part = early[...] + late
     edge_rows = part.astype(BF16).astype(F32).reshape(S + 1, 16, C + STATE)
 
     def tails(prompts):
@@ -363,7 +360,7 @@
     tails(range(G))
     if steps > 1:
         load_x(1).start()
-    gate_load = load(wg_hbm, wg, 7)
+    gate_load = load(wg_hbm, wg, 3)
     pl.semaphore_wait(barrier, len(peers))
 
     def halo_copy(k):
@@ -383,6 +380,19 @@
     def _():
         halo_copy(0).start()
 
+    taps[:, 0:F] = tv_ref[:, pl.ds(fcol, F)].astype(F32)
+    taps[:, F:C] = tk_ref[:, pl.ds(gcol, STATE)].astype(F32)
+    taps[:, C : C + STATE] = tq_ref[:, pl.ds(gcol, STATE)].astype(F32)
+    bias = bias_ref[...]
+    speed = jnp.exp(speed_ref[...])
+    square = jnp.zeros((128, 128 - HEADS), F32)
+
+    def columns(row, k):
+        full = jnp.concatenate([jnp.broadcast_to(row, (128, HEADS)), square], axis=1)
+        heads_t[k] = full.T[0:HEADS]
+        return heads_t[k, pl.ds(lead, heads), :]
+
+    bias_t, speed_t = columns(bias, 0), columns(speed, 1)
     tails(range(G, S))
 
     @pl.when(me < n - 1)
@@ -411,7 +421,6 @@
         newest_copy().start()
 
     new_raw = edge_rows[S]
-    first[0].wait()
     wall[:, 0:128] = jnp.concatenate(
         [ws[...], jnp.zeros((128 - heads, ws.shape[1]), BF16)], axis=0
     ).T
@@ -488,11 +497,16 @@
         return pltpu.make_async_remote_copy(
             log_out.at[here],
             log_in.at[here],
-            log_send.at[g],
+            log_send.at[0],
             log_recv.at[g],
             device_id=at(n - 1),
             device_id_type=MESH,
         )
+
+    def last_log_left(g):
+        @pl.when(g >= 1)
+        def _():
+            log_copy(g - 1).wait_send()
 
     def project(g):
         @pl.when(g == 0)
@@ -533,6 +547,7 @@
         def _():
             for q in range(G):
                 log_out[g * G + q] = log_own[g * G + q]
+            last_log_left(g)
             log_copy(g).start()
 
         for q in range(G):
@@ -615,6 +630,7 @@
 
     def pass_log(g):
         log_copy(g).wait_recv()
+        last_log_left(g)
         for q in range(G):
             log_out[g * G + q] = log_in[g * G + q] + log_own[g * G + q]
         log_copy(g).start()
@@ -785,8 +801,7 @@
             drain(s, True)
             drain(s, False)
             if s > 0:
-                for g in range(steps):
-                    log_copy(g).wait_send()
+                log_copy(steps - 1).wait_send()
 
     @pl.when(me < n - 1)
     def _():
@@ -870,6 +885,7 @@
             *[pltpu.VMEM(flat[i].shape, flat[i].dtype) for i in SMALL],
             pltpu.VMEM((S, L, D), BF16),
             pltpu.VMEM((S + 1, 16, D), BF16),
+            pltpu.VMEM(((S + 1) * 16, C + STATE), F32),
             pltpu.VMEM((D, 128 + C + STATE), BF16),
             pltpu.VMEM((heads, D), BF16),
             pltpu.VMEM((D, F), BF16),
@@ -892,13 +908,12 @@
             pltpu.VMEM((n * m - 1, 1, 128), F32),
             pltpu.VMEM((2 * heads, F), BF16),
             dma((16,)),
-            dma((2,)),
             dma((2, 2)),
             dma((2,)),
             dma((3, RING)),
             dma((2, S)),
             dma((2, steps)),
-            dma((steps,)),
+            dma((1,)),
             dma((steps,)),
             dma((2,)),
         ],

time: 42.6 us -> 42.3 us (level)
  no operation moved by 1% of the time
where the time goes in v5:
time: 42.3 us; the launch traced here: 42.1 us
  Pallas kernels  41.5 us (98%)
  between operations  0.64 us (2%)
    pallas_call x1, Pallas kernels, fused(): pl.pallas_call(lambda *refs: mixer_kernel(dims, *refs), out_shape=(pltpu....  40.7 us

profile of v5, /device:TPU:0, one launch (start us, length us, event | category | flops | bytes accessed | tf_op | source)
XLA Modules:
  0.0 42.1 jit_solution(12783001710285012809)
XLA Ops:
  0.6 40.7 %shard_map.158 = (bf16[12,128,128]{2,1,0:T(8,128)(2,1)S(1)}, bf16[12,128]{1,0:T(8,128)(2,1)S(1)}) custom-call(bf16[12,128,2048]{2,1,0:T(8,128)(2,1)} %refs_0_.1, bf16[12,2048]{1,0:T(8,128)(2,1)} %refs_1_.1, bf16[2048,512]{1,0:T(8,128)(2,1)} %refs_2_.1, bf16[2048,512]{1,0:T(8,128)(2,1)} %refs_3_.1, bf16[2048,256]{1,0:T(8,128)(2,1)} %refs_4_.1, ...), custom_call_target="tpu_custom_call" | custom-call | tf_op jit(solution)/shard_map/pallas_call | solution.py:876
  41.4 0.8 %shard_map.159 = (bf16[12,128,128]{2,1,0:T(8,128)(2,1)}, bf16[12,8,16]{2,1,0:T(8,128)(2,1)}) custom-call(bf16[12,128,128]{2,1,0:T(8,128)(2,1)S(1)} %get-tuple-element.6.refs_0_, bf16[12,128]{1,0:T(8,128)(2,1)S(1)} %get-tuple-element.7.refs_1_), custom_call_target="tpu_custom_call" | custom-call | tf_op jit(solution)/shard_map/pallas_call | solution.py:924

commit v6 on v5

--- a/solution.py
+++ b/solution.py
@@ -848,8 +848,8 @@
 LEAD, RELAY_LAG, FORWARD_AT = 1, 1, 2
 FAR, NEAR, FINAL = 0, 1, 2
 SMALL = (1, 7, 8, 9, 10, 11, 12, 13)
-RING, END_NEARS = 4, 2
-END_BEHIND, MID_BEHIND = 5, 2
+RING, END_NEARS = 2, 2
+END_BEHIND, MID_BEHIND = 5, 1
 
 
 def fused(*args):

time: 42.3 us -> 42.3 us (level)
  no operation moved by 1% of the time
where the time goes in v6:
time: 42.3 us; the launch traced here: 42.1 us
  Pallas kernels  41.4 us (98%)
  between operations  0.64 us (2%)
    pallas_call x1, Pallas kernels, fused(): pl.pallas_call(lambda *refs: mixer_kernel(dims, *refs), out_shape=(pltpu....  40.7 us

profile of v6, /device:TPU:0, one launch (start us, length us, event | category | flops | bytes accessed | tf_op | source)
XLA Modules:
  0.0 42.1 jit_solution(8314318664798558970)
XLA Ops:
  0.6 40.7 %shard_map.158 = (bf16[12,128,128]{2,1,0:T(8,128)(2,1)S(1)}, bf16[12,128]{1,0:T(8,128)(2,1)S(1)}) custom-call(bf16[12,128,2048]{2,1,0:T(8,128)(2,1)} %refs_0_.1, bf16[12,2048]{1,0:T(8,128)(2,1)} %refs_1_.1, bf16[2048,512]{1,0:T(8,128)(2,1)} %refs_2_.1, bf16[2048,512]{1,0:T(8,128)(2,1)} %refs_3_.1, bf16[2048,256]{1,0:T(8,128)(2,1)} %refs_4_.1, ...), custom_call_target="tpu_custom_call" | custom-call | tf_op jit(solution)/shard_map/pallas_call | solution.py:876
  41.3 0.8 %shard_map.159 = (bf16[12,128,128]{2,1,0:T(8,128)(2,1)}, bf16[12,8,16]{2,1,0:T(8,128)(2,1)}) custom-call(bf16[12,128,128]{2,1,0:T(8,128)(2,1)S(1)} %get-tuple-element.6.refs_0_, bf16[12,128]{1,0:T(8,128)(2,1)S(1)} %get-tuple-element.7.refs_1_), custom_call_target="tpu_custom_call" | custom-call | tf_op jit(solution)/shard_map/pallas_call | solution.py:924
